TPU v7x, 128 devices: a whole 4x4x4 slice. The times are simulated.
128 devices in a mesh: ra: 16 (over z, y), cb: 8 (over x, core).
Axes of the slice: x: 4, y: 4, z: 4, core: 2. Of those that a mesh axis runs over, the one named last changes fastest.
Arguments:
- tokens: bfloat16 [256, 3072], P(None, 'ra'), may hold values from -8 to 8, as said below
- first_gain: float32 [3072], P('ra'), may hold values from 0.1 to 1.9
- first_gate: float32 [3072, 8192], P('ra', 'cb'), may hold values from -0.109375 to 0.109375
- first_up: float32 [3072, 8192], P('ra', 'cb'), may hold values from -0.109375 to 0.109375
- first_down: float32 [8192, 3072], P('cb', 'ra'), may hold values from -0.0625 to 0.0625
- first_gate_scale: float32 [8192], P('cb'), may hold values from 0.5 to 2
- first_up_scale: float32 [8192], P('cb'), may hold values from 0.5 to 2
- first_down_scale: float32 [3072], P('ra'), may hold values from 0.5 to 2
- second_gain: float32 [3072], P('ra'), may hold values from 0.1 to 1.9
- second_gate: float32 [3072, 8192], P('ra', 'cb'), may hold values from -0.109375 to 0.109375
- second_up: float32 [3072, 8192], P('ra', 'cb'), may hold values from -0.109375 to 0.109375
- second_down: float32 [8192, 3072], P('cb', 'ra'), may hold values from -0.0625 to 0.0625
- second_gate_scale: float32 [8192], P('cb'), may hold values from 0.5 to 2
- second_up_scale: float32 [8192], P('cb'), may hold values from 0.5 to 2
- second_down_scale: float32 [3072], P('ra'), may hold values from 0.5 to 2
Outputs:
- mixed: bfloat16 [256, 3072], P(None, 'ra')
Inputs may be any that keep to these rules, and one draw needn't show every extreme that they name: The features come in groups of 64 with different magnitudes, and tokens differ in magnitude.
All inputs are finite; a program needn't handle non-finite values.
Results may differ from a plain program's by a relative error of at most 0.0093.
Values may be sent and summed in bfloat16 or wider, within the bound.
No kernel may reach another device: no remote copies, remote signals or barrier semaphores. Data moves between devices by JAX's collectives and lax.ppermute only.
A program may use at most 64 MiB of HBM per device.

v0:
```python
import functools

import jax
import jax.numpy as jnp
from jax import lax
from jax.experimental import pallas as pl
from jax.experimental.pallas import tpu as pltpu
from jax.sharding import PartitionSpec as P


D = 3072
SIDE = 4
WIDE = 1024
PIECE = 96
ORDER = (2, 1, 3)
X_ORDER = (2, 1, 3)
BF16 = jnp.bfloat16
F32 = jnp.float32
VMEM = pl.BlockSpec(memory_space=pltpu.VMEM)
HBM = pl.BlockSpec(memory_space=pltpu.HBM)
PARAMS = pltpu.CompilerParams(vmem_limit_bytes=12 << 20)


def rounded(x):
    return lax.reduce_precision(x, 8, 7)


def place_in_f():
    ra, cb = lax.axis_index("ra"), lax.axis_index("cb")
    return jnp.where(cb % 2 == 0, ra // SIDE, ra % SIDE)


def pairs_of(k, along_f):
    pairs = []
    for z in range(SIDE):
        for y in range(SIDE):
            for cb in range(8):
                if (cb % 2 == 0) == along_f:
                    to = (z ^ k, y)
                else:
                    to = (z, y ^ k)
                pairs.append(((z * SIDE + y) * 8 + cb, (to[0] * SIDE + to[1]) * 8 + cb))
    return pairs


def swapped(x, k, along_f):
    return lax.ppermute(x, ("ra", "cb"), pairs_of(k, along_f))


def other_core(x):
    return lax.ppermute(x, "cb", [(i, i ^ 1) for i in range(lax.axis_size("cb"))])


def sum_over_x(chip):
    sent = chip.astype(BF16)
    n = lax.axis_size("cb")
    others = {k: lax.ppermute(sent, "cb", [(i, i ^ 2 * k) for i in range(n)]).astype(F32) for k in X_ORDER}
    return (chip + others[2]) + (others[1] + others[3])


def packed_squares(squares):
    high = squares.astype(BF16).astype(F32)
    low = squares - high
    lane = lax.broadcasted_iota(jnp.int32, (8, 128), 1)
    tile = jnp.zeros((8, 128), F32)
    for k in range(squares.shape[0] // 8):
        tile = jnp.where(lane == 2 * k, high[8 * k : 8 * k + 8], tile)
        tile = jnp.where(lane == 2 * k + 1, low[8 * k : 8 * k + 8], tile)
    return tile.astype(BF16)


def whole_squares(tile):
    return tile + pltpu.roll(tile, 127, 1)


def turned_rows(stream_ref, turned):
    tokens = stream_ref.shape[1]
    rows = tokens // SIDE
    turned[0] = stream_ref[...].astype(F32).T
    place = place_in_f()
    for k in range(SIDE):
        at = pl.multiple_of((place ^ k) * rows, rows)
        turned[1, k * rows : (k + 1) * rows] = turned[0, pl.ds(at, rows)]
    return turned[1]


def write_products(stream, gain, pieces, out_refs):
    rows = stream.shape[0] // SIDE
    squares = jnp.sum(stream * stream, axis=1, keepdims=True)
    for k, out_ref in enumerate(out_refs):
        out_ref[len(pieces) * WIDE // 128 * rows :] = packed_squares(squares[k * rows : (k + 1) * rows])
    shaped = (stream * gain).astype(BF16)
    for c, piece in enumerate(pieces):
        part = jnp.dot(shaped, piece().astype(BF16), preferred_element_type=F32).astype(BF16)
        for k, out_ref in enumerate(out_refs):
            for n in range(WIDE // 128):
                at = (c * WIDE // 128 + n) * rows
                out_ref[at : at + rows] = part[k * rows : (k + 1) * rows, n * 128 : (n + 1) * 128]


def fetching_kernel(stream_ref, gain_ref, gate_ref, up_ref, *refs):
    small_refs, refs = refs[:5], refs[5:]
    out_refs, refs = refs[:SIDE], refs[SIDE:]
    half_ref, scales_ref, later_scales_ref, later_gain_ref, turned, stream_held, gain_held, held, sems, small_sems = refs
    targets = (
        stream_held,
        gain_held,
        scales_ref.at[0],
        scales_ref.at[1],
        later_scales_ref.at[0],
        later_scales_ref.at[1],
        later_gain_ref,
    )
    small = [
        pltpu.make_async_copy(ref, target, small_sems.at[k])
        for k, (ref, target) in enumerate(zip((stream_ref, gain_ref, *small_refs), targets, strict=True))
    ]
    for copy in small[:2]:
        copy.start()
    copies = [
        pltpu.make_async_copy(ref.at[pl.ds(at, PIECE)], held.at[n, pl.ds(at, PIECE)], sems.at[n, at // PIECE])
        for n, ref in enumerate((gate_ref, up_ref))
        for at in range(0, ref.shape[0], PIECE)
    ]
    for copy in copies:
        copy.start()
    for copy in small[2:]:
        copy.start()

    def piece(n, at):
        if at == 0:
            for copy in copies[n * len(copies) // 2 : (n + 1) * len(copies) // 2]:
                copy.wait()
        return held[n, :, at : at + WIDE]

    small[0].wait()
    stream = turned_rows(stream_held, turned)
    near = pl.multiple_of(lax.axis_index("cb") % 2 * half_ref.shape[1], half_ref.shape[1])
    half_ref[...] = stream_held[:, pl.ds(near, half_ref.shape[1])]
    small[1].wait()
    pieces = [functools.partial(piece, n, at) for n in range(2) for at in range(0, held.shape[2], WIDE)]
    write_products(stream, gain_held[...], pieces, out_refs)
    for copy in small[2:]:
        copy.wait()


def products_kernel(stream_ref, gain_ref, *refs):
    w_refs, (*out_refs, turned) = refs[: -SIDE - 1], refs[-SIDE - 1 :]

    def piece(ref, at):
        return ref[:, at : at + WIDE]

    pieces = [functools.partial(piece, ref, at) for ref in w_refs for at in range(0, ref.shape[1], WIDE)]
    write_products(turned_rows(stream_ref, turned), gain_ref[...], pieces, out_refs)


def products(stream, gain, weights, small=()):
    features, tokens = stream.shape
    columns = sum(w.shape[1] for w in weights)
    units = weights[0].shape[1]
    scratch = [
        pltpu.VMEM((2, tokens, features), F32),
        pltpu.VMEM((features, tokens), BF16),
        pltpu.VMEM((1, features), F32),
        pltpu.VMEM((2, features, units), F32),
        pltpu.SemaphoreType.DMA((2, features // PIECE)),
        pltpu.SemaphoreType.DMA((7,)),
    ]
    operands = [stream, gain, *weights, *small]
    rows = tokens // SIDE
    outs = [jax.ShapeDtypeStruct((columns // 128 * rows + 8, 128), BF16)] * SIDE
    if small:
        operands = [pltpu.with_memory_space_constraint(x, pltpu.HBM) for x in operands]
        outs += [jax.ShapeDtypeStruct((features, tokens // 2), BF16)]
        outs += [jax.ShapeDtypeStruct((2, 1, units), F32)] * 2 + [jax.ShapeDtypeStruct((1, features), F32)]
    outs = pl.pallas_call(
        fetching_kernel if small else products_kernel,
        out_shape=outs,
        in_specs=[HBM if small else VMEM] * len(operands),
        out_specs=[VMEM] * len(outs),
        scratch_shapes=scratch if small else scratch[:1],
        compiler_params=PARAMS,
        cost_estimate=pl.CostEstimate(
            flops=2 * tokens * features * columns, bytes_accessed=4 * features * columns, transcendentals=0
        ),
    )(*operands)
    return outs[:SIDE], outs[SIDE:]


def total_of(refs):
    return sum(ref[...].astype(F32) for ref in refs[1:]) + refs[0][...].astype(F32)


def add_kernel(*refs):
    *in_refs, out_ref = refs
    end = out_ref.shape[0] - 8
    total = total_of(in_refs)
    out_ref[:end] = total[:end].astype(BF16)
    squares = whole_squares(total[end:])
    high = squares.astype(BF16).astype(F32)
    lane = lax.broadcasted_iota(jnp.int32, squares.shape, 1)
    out_ref[end:] = jnp.where(lane % 2 == 0, high, pltpu.roll(squares - high, 1, 1)).astype(BF16)


def hidden_kernel(count, *refs):
    in_refs, scales_refs, out_ref = refs[:SIDE], refs[SIDE : SIDE + count], refs[-1]
    rows, units = out_ref.shape
    each = units // count
    total = total_of(in_refs)
    inverse = lax.rsqrt(whole_squares(total[2 * units // 128 * rows :]) / D + 1e-06)
    inverse = jnp.concatenate([inverse[:, 2 * k : 2 * k + 1] for k in range(rows // 8)])
    for n in range(units // 128):
        scales_ref, at = scales_refs[n * 128 // each], n * 128 % each
        gate = inverse * scales_ref[0, :, at : at + 128] * total[n * rows : (n + 1) * rows]
        m = n + units // 128
        up = inverse * scales_ref[1, :, at : at + 128] * total[m * rows : (m + 1) * rows]
        out_ref[:, n * 128 : (n + 1) * 128] = (gate / (1.0 + jnp.exp(-gate)) * up).astype(BF16)


def down_kernel(count, *refs):
    in_refs, w_refs, (*out_refs, hidden) = refs[:SIDE], refs[SIDE : SIDE + count], refs[SIDE + count :]
    rows = in_refs[0].shape[0]
    tokens = rows * SIDE
    place = place_in_f()
    turn = lax.axis_index("cb") % 2 * (SIDE // 2) if len(out_refs) == 2 else 0
    for k, ref in enumerate(in_refs):
        at = pl.multiple_of(((place ^ k) + turn) % SIDE * rows, rows)
        hidden[pl.ds(at, rows)] = ref[...]
    each = hidden.shape[1] // count
    for n, out_ref in enumerate(out_refs):
        wide = tokens // len(out_refs)
        parts = [
            lax.dot_general(
                w_ref[...].astype(BF16),
                hidden[n * wide : (n + 1) * wide, k * each : (k + 1) * each],
                (((1,), (1,)), ((), ())),
                preferred_element_type=F32,
            )
            for k, w_ref in enumerate(w_refs)
        ]
        out_ref[...] = functools.reduce(jnp.add, parts).astype(BF16)


def call(kernel, shapes, *operands, scratch=(), flops=0):
    return pl.pallas_call(
        kernel,
        out_shape=[jax.ShapeDtypeStruct(shape, BF16) for shape in shapes],
        in_specs=[VMEM] * len(operands),
        out_specs=[VMEM] * len(shapes),
        scratch_shapes=scratch,
        compiler_params=PARAMS,
        cost_estimate=pl.CostEstimate(
            flops=flops or 8 * operands[0].size,
            bytes_accessed=sum(x.size * x.dtype.itemsize for x in operands),
            transcendentals=0,
        ),
    )(*operands)


def hidden_blocks(mine, scales):
    peers = [swapped(mine, k, False) for k in ORDER]
    units = sum(x.shape[2] for x in scales)
    rows = mine.shape[0] // (2 * units // 128)
    kernel = functools.partial(hidden_kernel, len(scales))
    (hidden,) = call(kernel, [(rows, units)], mine, *peers, *scales)
    others = {k: swapped(hidden, k, True) for k in ORDER}
    return hidden, others[1], others[2], others[3]


def down_products(blocks, weights, outs):
    rows, units = blocks[0].shape
    tokens, features = rows * SIDE, weights[0].shape[1]
    return call(
        functools.partial(down_kernel, len(weights)),
        [(features, tokens // outs)] * outs,
        *blocks,
        *(w.T for w in weights),
        scratch=[pltpu.VMEM((tokens, units), BF16)],
        flops=2 * tokens * units * features,
    )


def step_result(stream, down_scale, down):
    return (stream.astype(F32) + 0.5 * down_scale[:, None] * down).astype(BF16)


def body(
    tokens,
    first_gain,
    first_gate,
    first_up,
    first_down,
    first_gate_scale,
    first_up_scale,
    first_down_scale,
    second_gain,
    second_gate,
    second_up,
    second_down,
    second_gate_scale,
    second_up_scale,
    second_down_scale,
):
    small = (first_gate_scale, first_up_scale, second_gate_scale, second_up_scale, second_gain)
    blocks, (half, scales, later_scales, later_gain) = products(
        tokens.T, first_gain[None, :], (first_gate, first_up), [x[None, :] for x in small]
    )
    received = [swapped(blocks[k], k, True) for k in ORDER]
    theirs = [other_core(x) for x in (second_gate, second_up, second_down.T, later_scales)]
    received, theirs = lax.optimization_barrier((received, theirs))
    their_gate, their_up, their_down, their_scales = theirs
    (mine,) = call(add_kernel, [blocks[0].shape], blocks[0], *received)
    near, far = down_products(hidden_blocks(mine, [scales]), [first_down], 2)
    chip = rounded(near.astype(F32) + other_core(far).astype(F32))
    middle = step_result(half, first_down_scale, sum_over_x(chip))

    blocks, _ = products(middle, later_gain, (second_gate, their_gate, second_up, their_up))
    received = [swapped(blocks[k], k, True) for k in ORDER]
    (mine,) = call(add_kernel, [blocks[0].shape], blocks[0], *received)
    hidden = hidden_blocks(mine, [later_scales, their_scales])
    (down,) = down_products(hidden, [second_down, their_down.T], 1)
    mixed = step_result(middle, second_down_scale, sum_over_x(down.astype(F32)))
    other = other_core(mixed)
    first = lax.axis_index("cb") % 2 == 0
    both = jnp.where(first, jnp.concatenate([mixed, other], axis=1), jnp.concatenate([other, mixed], axis=1))
    return both.T


def solution(mesh):
    one = (P("ra"), P("ra", "cb"), P("ra", "cb"), P("cb", "ra"), P("cb"), P("cb"), P("ra"))
    return jax.shard_map(
        body, mesh=mesh, in_specs=(P(None, "ra"), *one, *one), out_specs=P(None, "ra"), check_vma=False
    )
```

profile of v0, /device:TPU:1, one launch (start us, length us, event | category | flops | bytes accessed | tf_op | source)
XLA Modules:
  0.0 95.0 jit_solution(8196440045056120179)
XLA Ops:
  0.0 1.4 %collective-permute-start.5 = (f32[192,1024]{1,0:T(8,128)}, f32[192,1024]{1,0:T(8,128)S(1)}, u32[]{:S(2)}, u32[]{:S(2)}) collective-permute-start(f32[192,1024]{1,0:T(8,128)} %bitcast.12), channel_id=1, source_target_pairs={{0,1},{1,0},{2,3},{3,2},{4,5},{5,4},{6,7},{7,6},{8,9},{9,8},{10,11... | collective-permute-start | bytes 2359304 | tf_op jit(solution)/shard_map/ppermute | solution.py:51
  1.4 0.5 collective-permute-start.4
  1.9 2.0 %shard_map.145 = (bf16[1032,128]{1,0:T(8,128)(2,1)S(1)}, bf16[1032,128]{1,0:T(8,128)(2,1)S(1)}, bf16[1032,128]{1,0:T(8,128)(2,1)S(1)}, bf16[1032,128]{1,0:T(8,12...) custom-call(bf16[192,256]{1,0:T(8,128)(2,1)} %bitcast.14, ...), custom_call_target="tpu_custom_call" | custom-call | flops 201326592 | bytes 1572864 | tf_op jit(solution)/shard_map/pallas_call | solution.py:176
  3.9 3.1 %collective-permute-start = (bf16[1032,128]{1,0:T(8,128)(2,1)S(1)}, bf16[1032,128]{1,0:T(8,128)(2,1)S(1)}, u32[]{:S(2)}, u32[]{:S(2)}) collective-permute-start(bf16[1032,128]{1,0:T(8,128)(2,1)S(1)} %get-tuple-element.28), channel_id=1, source_target_pairs={{0,64},{1,17},{2,66},{3,19},{4,68},{5,21},{6,70},{7,23},{8,72},{9,... | collective-permute-start | bytes 792584 | tf_op jit(solution)/shard_map/ppermute | solution.py:47
  7.0 1.0 %collective-permute-start.6 = (f32[2,1,1024]{2,1,0:T(1,128)S(1)}, f32[2,1,1024]{2,1,0:T(1,128)S(1)}, u32[]{:S(2)}, u32[]{:S(2)}) collective-permute-start(f32[2,1,1024]{2,1,0:T(1,128)S(1)} %get-tuple-element.31.refs_4_), channel_id=1, source_target_pairs={{0,1},{1,0},{2,3},{3,2},{4,5},{5,4},{6,7},{7,6},{8,9},{9,8},{10,11... | collective-permute-start | bytes 24584 | tf_op jit(solution)/shard_map/ppermute | solution.py:51
  8.0 0.8 collective-permute-done.6.refs_5_
  8.8 1.3 %collective-permute-start.1 = (bf16[1032,128]{1,0:T(8,128)(2,1)S(1)}, bf16[1032,128]{1,0:T(8,128)(2,1)S(1)}, u32[]{:S(2)}, u32[]{:S(2)}) collective-permute-start(bf16[1032,128]{1,0:T(8,128)(2,1)S(1)} %get-tuple-element.29), channel_id=1, source_target_pairs={{0,32},{1,9},{2,34},{3,11},{4,36},{5,13},{6,38},{7,15},{8,40},{9,1... | collective-permute-start | bytes 792584 | tf_op jit(solution)/shard_map/ppermute | solution.py:47
  10.1 1.0 %collective-permute-done.refs_1_ = bf16[1032,128]{1,0:T(8,128)(2,1)S(1)} collective-permute-done((bf16[1032,128]{1,0:T(8,128)(2,1)S(1)}, bf16[1032,128]{1,0:T(8,128)(2,1)S(1)}, u32[]{:S(2)}, u32[]{:S(2)}) %collective-permute-start) | collective-permute-done | bytes 264224 | tf_op jit(solution)/shard_map/ppermute | solution.py:47
  11.1 2.8 %collective-permute-start.2 = (bf16[1032,128]{1,0:T(8,128)(2,1)S(1)}, bf16[1032,128]{1,0:T(8,128)(2,1)S(1)}, u32[]{:S(2)}, u32[]{:S(2)}) collective-permute-start(bf16[1032,128]{1,0:T(8,128)(2,1)S(1)} %get-tuple-element.30), channel_id=1, source_target_pairs={{0,96},{1,25},{2,98},{3,27},{4,100},{5,29},{6,102},{7,31},{8,104},... | collective-permute-start | bytes 792584 | tf_op jit(solution)/shard_map/ppermute | solution.py:47
  13.9 0.5 collective-permute-done.1.refs_2_
  14.3 3.6 %collective-permute-done.2.refs_3_ = bf16[1032,128]{1,0:T(8,128)(2,1)S(1)} collective-permute-done((bf16[1032,128]{1,0:T(8,128)(2,1)S(1)}, bf16[1032,128]{1,0:T(8,128)(2,1)S(1)}, u32[]{:S(2)}, u32[]{:S(2)}) %collective-permute-start.2) | collective-permute-done | bytes 264224 | tf_op jit(solution)/shard_map/ppermute | solution.py:47
  17.9 0.3 shard_map.146.refs_0_
  18.2 0.0 copy-start
  18.2 3.1 %collective-permute-start.7 = (bf16[1032,128]{1,0:T(8,128)(2,1)S(1)}, bf16[1032,128]{1,0:T(8,128)(2,1)S(1)}, u32[]{:S(2)}, u32[]{:S(2)}) collective-permute-start(bf16[1032,128]{1,0:T(8,128)(2,1)S(1)} %shard_map.146.refs_0_), channel_id=1, source_target_pairs={{0,16},{1,65},{2,18},{3,67},{4,20},{5,69},{6,22},{7,71},{8,24},{9,... | collective-permute-start | bytes 792584 | tf_op jit(solution)/shard_map/ppermute | solution.py:47
  21.3 1.3 %collective-permute-start.8 = (bf16[1032,128]{1,0:T(8,128)(2,1)S(1)}, bf16[1032,128]{1,0:T(8,128)(2,1)S(1)}, u32[]{:S(2)}, u32[]{:S(2)}) collective-permute-start(bf16[1032,128]{1,0:T(8,128)(2,1)S(1)} %shard_map.146.refs_0_), channel_id=1, source_target_pairs={{0,8},{1,33},{2,10},{3,35},{4,12},{5,37},{6,14},{7,39},{8,0},{9,41... | collective-permute-start | bytes 792584 | tf_op jit(solution)/shard_map/ppermute | solution.py:47
  22.7 2.5 %collective-permute-done.7.refs_1_ = bf16[1032,128]{1,0:T(8,128)(2,1)S(1)} collective-permute-done((bf16[1032,128]{1,0:T(8,128)(2,1)S(1)}, bf16[1032,128]{1,0:T(8,128)(2,1)S(1)}, u32[]{:S(2)}, u32[]{:S(2)}) %collective-permute-start.7) | collective-permute-done | bytes 264224 | tf_op jit(solution)/shard_map/ppermute | solution.py:47
  25.1 4.5 %collective-permute-done.8.refs_2_ = bf16[1032,128]{1,0:T(8,128)(2,1)S(1)} collective-permute-done((bf16[1032,128]{1,0:T(8,128)(2,1)S(1)}, bf16[1032,128]{1,0:T(8,128)(2,1)S(1)}, u32[]{:S(2)}, u32[]{:S(2)}) %collective-permute-start.8) | collective-permute-done | bytes 264224 | tf_op jit(solution)/shard_map/ppermute | solution.py:47
  29.6 0.4 shard_map.147.refs_0_
  30.0 0.1 collective-permute-start.10
  30.1 3.8 %collective-permute-start.11 = (bf16[64,1024]{1,0:T(8,128)(2,1)S(1)}, bf16[64,1024]{1,0:T(8,128)(2,1)S(1)}, u32[]{:S(2)}, u32[]{:S(2)}) collective-permute-start(bf16[64,1024]{1,0:T(8,128)(2,1)S(1)} %shard_map.147.refs_0_), channel_id=1, source_target_pairs={{0,64},{1,17},{2,66},{3,19},{4,68},{5,21},{6,70},{7,23},{8,72},{9,... | collective-permute-start | bytes 393224 | tf_op jit(solution)/shard_map/ppermute | solution.py:47
  33.9 3.8 %collective-permute-done.11.refs_2_ = bf16[64,1024]{1,0:T(8,128)(2,1)S(1)} collective-permute-done((bf16[64,1024]{1,0:T(8,128)(2,1)S(1)}, bf16[64,1024]{1,0:T(8,128)(2,1)S(1)}, u32[]{:S(2)}, u32[]{:S(2)}) %collective-permute-start.11) | collective-permute-done | bytes 131104 | tf_op jit(solution)/shard_map/ppermute | solution.py:47
  37.7 1.4 %collective-permute-done.12.refs_3_ = bf16[64,1024]{1,0:T(8,128)(2,1)S(1)} collective-permute-done((bf16[64,1024]{1,0:T(8,128)(2,1)S(1)}, bf16[64,1024]{1,0:T(8,128)(2,1)S(1)}, u32[]{:S(2)}, u32[]{:S(2)}) %collective-permute-start.12) | collective-permute-done | bytes 131104 | tf_op jit(solution)/shard_map/ppermute | solution.py:47
  39.1 0.4 shard_map.148
  39.6 4.6 %collective-permute-start.13 = (bf16[192,128]{1,0:T(8,128)(2,1)S(1)}, bf16[192,128]{1,0:T(8,128)(2,1)S(1)}, u32[]{:S(2)}, u32[]{:S(2)}) collective-permute-start(bf16[192,128]{1,0:T(8,128)(2,1)S(1)} %get-tuple-element.37), channel_id=1, source_target_pairs={{0,1},{1,0},{2,3},{3,2},{4,5},{5,4},{6,7},{7,6},{8,9},{9,8},{10,11... | collective-permute-start | bytes 147464 | tf_op jit(solution)/shard_map/ppermute | solution.py:51
  44.1 0.9 collective-permute-done.13
  45.0 2.8 %collective-permute-start.14 = (bf16[192,128]{1,0:T(8,128)(2,1)S(1)}, bf16[192,128]{1,0:T(8,128)(2,1)S(1)}, u32[]{:S(2)}, u32[]{:S(2)}) collective-permute-start(bf16[192,128]{1,0:T(8,128)(2,1)S(1)} %fusion.1), channel_id=1, source_target_pairs={{0,4},{1,5},{2,6},{3,7},{4,0},{5,1},{6,2},{7,3},{8,12},{9,13},{10,... | collective-permute-start | bytes 147464 | tf_op jit(solution)/shard_map/ppermute | solution.py:57
  47.9 0.3 collective-permute-start.15
  48.2 0.6 collective-permute-start.16
  48.7 0.8 collective-permute-done.14
  49.6 1.4 %collective-permute-done.15 = bf16[192,128]{1,0:T(8,128)(2,1)S(1)} collective-permute-done((bf16[192,128]{1,0:T(8,128)(2,1)S(1)}, bf16[192,128]{1,0:T(8,128)(2,1)S(1)}, u32[]{:S(2)}, u32[]{:S(2)}) %collective-permute-start.15) | collective-permute-done | bytes 49184 | tf_op jit(solution)/shard_map/ppermute | solution.py:57
  51.0 1.3 %collective-permute-done.16 = bf16[192,128]{1,0:T(8,128)(2,1)S(1)} collective-permute-done((bf16[192,128]{1,0:T(8,128)(2,1)S(1)}, bf16[192,128]{1,0:T(8,128)(2,1)S(1)}, u32[]{:S(2)}, u32[]{:S(2)}) %collective-permute-start.16) | collective-permute-done | bytes 49184 | tf_op jit(solution)/shard_map/ppermute | solution.py:57
  52.3 0.1 add_convert_fusion.1.stream_ref
  52.4 0.5 shard_map.149
  53.0 2.2 %collective-permute-start.17 = (bf16[1032,128]{1,0:T(8,128)(2,1)S(1)}, bf16[1032,128]{1,0:T(8,128)(2,1)S(1)}, u32[]{:S(2)}, u32[]{:S(2)}) collective-permute-start(bf16[1032,128]{1,0:T(8,128)(2,1)S(1)} %get-tuple-element.42), channel_id=1, source_target_pairs={{0,64},{1,17},{2,66},{3,19},{4,68},{5,21},{6,70},{7,23},{8,72},{9,... | collective-permute-start | bytes 792584 | tf_op jit(solution)/shard_map/ppermute | solution.py:47
  55.2 0.4 collective-permute-start.18
  55.6 1.0 %collective-permute-start.19 = (bf16[1032,128]{1,0:T(8,128)(2,1)S(1)}, bf16[1032,128]{1,0:T(8,128)(2,1)S(1)}, u32[]{:S(2)}, u32[]{:S(2)}) collective-permute-start(bf16[1032,128]{1,0:T(8,128)(2,1)S(1)} %get-tuple-element.44), channel_id=1, source_target_pairs={{0,96},{1,25},{2,98},{3,27},{4,100},{5,29},{6,102},{7,31},{8,104},... | collective-permute-start | bytes 792584 | tf_op jit(solution)/shard_map/ppermute | solution.py:47
  56.6 3.4 %collective-permute-done.17.refs_1_ = bf16[1032,128]{1,0:T(8,128)(2,1)S(1)} collective-permute-done((bf16[1032,128]{1,0:T(8,128)(2,1)S(1)}, bf16[1032,128]{1,0:T(8,128)(2,1)S(1)}, u32[]{:S(2)}, u32[]{:S(2)}) %collective-permute-start.17) | collective-permute-done | bytes 264224 | tf_op jit(solution)/shard_map/ppermute | solution.py:47
  60.1 2.4 %collective-permute-done.18.refs_2_ = bf16[1032,128]{1,0:T(8,128)(2,1)S(1)} collective-permute-done((bf16[1032,128]{1,0:T(8,128)(2,1)S(1)}, bf16[1032,128]{1,0:T(8,128)(2,1)S(1)}, u32[]{:S(2)}, u32[]{:S(2)}) %collective-permute-start.18) | collective-permute-done | bytes 264224 | tf_op jit(solution)/shard_map/ppermute | solution.py:47
  62.5 0.4 collective-permute-done.19.refs_3_
  62.9 0.3 shard_map.150.refs_0_
  63.2 0.0 copy-start.1
  63.2 0.1 collective-permute-start.20
  63.3 0.3 collective-permute-start.21
  63.6 2.9 %collective-permute-start.22 = (bf16[1032,128]{1,0:T(8,128)(2,1)S(1)}, bf16[1032,128]{1,0:T(8,128)(2,1)S(1)}, u32[]{:S(2)}, u32[]{:S(2)}) collective-permute-start(bf16[1032,128]{1,0:T(8,128)(2,1)S(1)} %shard_map.150.refs_0_), channel_id=1, source_target_pairs={{0,24},{1,97},{2,26},{3,99},{4,28},{5,101},{6,30},{7,103},{8,16},{... | collective-permute-start | bytes 792584 | tf_op jit(solution)/shard_map/ppermute | solution.py:47
  66.6 3.6 %collective-permute-done.20.refs_1_ = bf16[1032,128]{1,0:T(8,128)(2,1)S(1)} collective-permute-done((bf16[1032,128]{1,0:T(8,128)(2,1)S(1)}, bf16[1032,128]{1,0:T(8,128)(2,1)S(1)}, u32[]{:S(2)}, u32[]{:S(2)}) %collective-permute-start.20) | collective-permute-done | bytes 264224 | tf_op jit(solution)/shard_map/ppermute | solution.py:47
  70.1 0.1 collective-permute-done.21.refs_2_
  70.2 2.9 %collective-permute-done.22.refs_3_ = bf16[1032,128]{1,0:T(8,128)(2,1)S(1)} collective-permute-done((bf16[1032,128]{1,0:T(8,128)(2,1)S(1)}, bf16[1032,128]{1,0:T(8,128)(2,1)S(1)}, u32[]{:S(2)}, u32[]{:S(2)}) %collective-permute-start.22) | collective-permute-done | bytes 264224 | tf_op jit(solution)/shard_map/ppermute | solution.py:47
  73.2 0.4 shard_map.151.refs_0_
  73.6 0.0 copy-start.5
  73.6 1.1 %collective-permute-start.23 = (bf16[32,2048]{1,0:T(8,128)(2,1)S(1)}, bf16[32,2048]{1,0:T(8,128)(2,1)S(1)}, u32[]{:S(2)}, u32[]{:S(2)}) collective-permute-start(bf16[32,2048]{1,0:T(8,128)(2,1)S(1)} %shard_map.151.refs_0_), channel_id=1, source_target_pairs={{0,32},{1,9},{2,34},{3,11},{4,36},{5,13},{6,38},{7,15},{8,40},{9,1... | collective-permute-start | bytes 393224 | tf_op jit(solution)/shard_map/ppermute | solution.py:47
  74.7 2.1 %collective-permute-start.24 = (bf16[32,2048]{1,0:T(8,128)(2,1)S(1)}, bf16[32,2048]{1,0:T(8,128)(2,1)S(1)}, u32[]{:S(2)}, u32[]{:S(2)}) collective-permute-start(bf16[32,2048]{1,0:T(8,128)(2,1)S(1)} %shard_map.151.refs_0_), channel_id=1, source_target_pairs={{0,64},{1,17},{2,66},{3,19},{4,68},{5,21},{6,70},{7,23},{8,72},{9,... | collective-permute-start | bytes 393224 | tf_op jit(solution)/shard_map/ppermute | solution.py:47
  76.8 0.7 collective-permute-start.25
  77.5 3.1 %collective-permute-done.24.refs_2_ = bf16[32,2048]{1,0:T(8,128)(2,1)S(1)} collective-permute-done((bf16[32,2048]{1,0:T(8,128)(2,1)S(1)}, bf16[32,2048]{1,0:T(8,128)(2,1)S(1)}, u32[]{:S(2)}, u32[]{:S(2)}) %collective-permute-start.24) | collective-permute-done | bytes 131104 | tf_op jit(solution)/shard_map/ppermute | solution.py:47
  80.6 1.4 %collective-permute-done.25.refs_3_ = bf16[32,2048]{1,0:T(8,128)(2,1)S(1)} collective-permute-done((bf16[32,2048]{1,0:T(8,128)(2,1)S(1)}, bf16[32,2048]{1,0:T(8,128)(2,1)S(1)}, u32[]{:S(2)}, u32[]{:S(2)}) %collective-permute-start.25) | collective-permute-done | bytes 131104 | tf_op jit(solution)/shard_map/ppermute | solution.py:47
  82.0 0.4 shard_map.152
  82.4 1.4 %collective-permute-start.26 = (bf16[192,128]{1,0:T(8,128)(2,1)S(1)}, bf16[192,128]{1,0:T(8,128)(2,1)S(1)}, u32[]{:S(2)}, u32[]{:S(2)}) collective-permute-start(bf16[192,128]{1,0:T(8,128)(2,1)S(1)} %shard_map.152), channel_id=1, source_target_pairs={{0,4},{1,5},{2,6},{3,7},{4,0},{5,1},{6,2},{7,3},{8,12},{9,13},{10,... | collective-permute-start | bytes 147464 | tf_op jit(solution)/shard_map/ppermute | solution.py:57
  83.9 0.6 collective-permute-start.27
  84.4 1.3 %collective-permute-start.28 = (bf16[192,128]{1,0:T(8,128)(2,1)S(1)}, bf16[192,128]{1,0:T(8,128)(2,1)S(1)}, u32[]{:S(2)}, u32[]{:S(2)}) collective-permute-start(bf16[192,128]{1,0:T(8,128)(2,1)S(1)} %shard_map.152), channel_id=1, source_target_pairs={{0,6},{1,7},{2,4},{3,5},{4,2},{5,3},{6,0},{7,1},{8,14},{9,15},{10,... | collective-permute-start | bytes 147464 | tf_op jit(solution)/shard_map/ppermute | solution.py:57
  85.8 1.2 %collective-permute-done.26 = bf16[192,128]{1,0:T(8,128)(2,1)S(1)} collective-permute-done((bf16[192,128]{1,0:T(8,128)(2,1)S(1)}, bf16[192,128]{1,0:T(8,128)(2,1)S(1)}, u32[]{:S(2)}, u32[]{:S(2)}) %collective-permute-start.26) | collective-permute-done | bytes 49184 | tf_op jit(solution)/shard_map/ppermute | solution.py:57
  87.0 1.6 %collective-permute-done.28 = bf16[192,128]{1,0:T(8,128)(2,1)S(1)} collective-permute-done((bf16[192,128]{1,0:T(8,128)(2,1)S(1)}, bf16[192,128]{1,0:T(8,128)(2,1)S(1)}, u32[]{:S(2)}, u32[]{:S(2)}) %collective-permute-start.28) | collective-permute-done | bytes 49184 | tf_op jit(solution)/shard_map/ppermute | solution.py:57
  88.6 0.1 add_convert_fusion
  88.7 4.8 %collective-permute-start.29 = (bf16[192,128]{1,0:T(8,128)(2,1)S(1)}, bf16[192,128]{1,0:T(8,128)(2,1)S(1)}, u32[]{:S(2)}, u32[]{:S(2)}) collective-permute-start(bf16[192,128]{1,0:T(8,128)(2,1)S(1)} %add_convert_fusion), channel_id=1, source_target_pairs={{0,1},{1,0},{2,3},{3,2},{4,5},{5,4},{6,7},{7,6},{8,9},{9,8},{10,11... | collective-permute-start | bytes 147464 | tf_op jit(solution)/shard_map/ppermute | solution.py:51
  93.4 0.9 collective-permute-done.29
  94.3 0.7 fusion
  (22 shorter events, 0.1 us)
Async XLA Ops:
  0.0 17.9 %collective-permute-start.5 = (f32[192,1024]{1,0:T(8,128)}, f32[192,1024]{1,0:T(8,128)S(1)}, u32[]{:S(2)}, u32[]{:S(2)}) collective-permute-start(f32[192,1024]{1,0:T(8,128)} %bitcast.12), channel_id=1, source_target_pairs={{0,1},{1,0},{2,3},{3,2},{4,5},{5,4},{6,7},{7,6},{8,9},{9,8},{10,11... | collective-permute-start | bytes 2359304 | tf_op jit(solution)/shard_map/ppermute | solution.py:51
  1.4 16.6 %collective-permute-start.3 = (f32[192,1024]{1,0:T(8,128)}, f32[192,1024]{1,0:T(8,128)S(1)}, u32[]{:S(2)}, u32[]{:S(2)}) collective-permute-start(f32[192,1024]{1,0:T(8,128)} %refs_0_.1), channel_id=1, source_target_pairs={{0,1},{1,0},{2,3},{3,2},{4,5},{5,4},{6,7},{7,6},{8,9},{9,8},{10,11... | collective-permute-start | bytes 2359304 | tf_op jit(solution)/shard_map/ppermute | solution.py:51
  1.4 16.6 %collective-permute-start.4 = (f32[192,1024]{1,0:T(8,128)}, f32[192,1024]{1,0:T(8,128)S(1)}, u32[]{:S(2)}, u32[]{:S(2)}) collective-permute-start(f32[192,1024]{1,0:T(8,128)} %refs_2_.1), channel_id=1, source_target_pairs={{0,1},{1,0},{2,3},{3,2},{4,5},{5,4},{6,7},{7,6},{8,9},{9,8},{10,11... | collective-permute-start | bytes 2359304 | tf_op jit(solution)/shard_map/ppermute | solution.py:51
  3.9 7.2 %collective-permute-start = (bf16[1032,128]{1,0:T(8,128)(2,1)S(1)}, bf16[1032,128]{1,0:T(8,128)(2,1)S(1)}, u32[]{:S(2)}, u32[]{:S(2)}) collective-permute-start(bf16[1032,128]{1,0:T(8,128)(2,1)S(1)} %get-tuple-element.28), channel_id=1, source_target_pairs={{0,64},{1,17},{2,66},{3,19},{4,68},{5,21},{6,70},{7,23},{8,72},{9,... | collective-permute-start | bytes 792584 | tf_op jit(solution)/shard_map/ppermute | solution.py:47
  7.0 1.8 %collective-permute-start.6 = (f32[2,1,1024]{2,1,0:T(1,128)S(1)}, f32[2,1,1024]{2,1,0:T(1,128)S(1)}, u32[]{:S(2)}, u32[]{:S(2)}) collective-permute-start(f32[2,1,1024]{2,1,0:T(1,128)S(1)} %get-tuple-element.31.refs_4_), channel_id=1, source_target_pairs={{0,1},{1,0},{2,3},{3,2},{4,5},{5,4},{6,7},{7,6},{8,9},{9,8},{10,11... | collective-permute-start | bytes 24584 | tf_op jit(solution)/shard_map/ppermute | solution.py:51
  8.8 5.5 %collective-permute-start.1 = (bf16[1032,128]{1,0:T(8,128)(2,1)S(1)}, bf16[1032,128]{1,0:T(8,128)(2,1)S(1)}, u32[]{:S(2)}, u32[]{:S(2)}) collective-permute-start(bf16[1032,128]{1,0:T(8,128)(2,1)S(1)} %get-tuple-element.29), channel_id=1, source_target_pairs={{0,32},{1,9},{2,34},{3,11},{4,36},{5,13},{6,38},{7,15},{8,40},{9,1... | collective-permute-start | bytes 792584 | tf_op jit(solution)/shard_map/ppermute | solution.py:47
  11.1 6.9 %collective-permute-start.2 = (bf16[1032,128]{1,0:T(8,128)(2,1)S(1)}, bf16[1032,128]{1,0:T(8,128)(2,1)S(1)}, u32[]{:S(2)}, u32[]{:S(2)}) collective-permute-start(bf16[1032,128]{1,0:T(8,128)(2,1)S(1)} %get-tuple-element.30), channel_id=1, source_target_pairs={{0,96},{1,25},{2,98},{3,27},{4,100},{5,29},{6,102},{7,31},{8,104},... | collective-permute-start | bytes 792584 | tf_op jit(solution)/shard_map/ppermute | solution.py:47
  18.2 20.9 %copy-start = (f32[1024,192]{0,1:T(8,128)S(1)}, f32[1024,192]{0,1:T(8,128)}, u32[]{:S(2)}) copy-start(f32[1024,192]{0,1:T(8,128)} %param.19) | copy-start | bytes 2359300
  18.2 6.9 %collective-permute-start.7 = (bf16[1032,128]{1,0:T(8,128)(2,1)S(1)}, bf16[1032,128]{1,0:T(8,128)(2,1)S(1)}, u32[]{:S(2)}, u32[]{:S(2)}) collective-permute-start(bf16[1032,128]{1,0:T(8,128)(2,1)S(1)} %shard_map.146.refs_0_), channel_id=1, source_target_pairs={{0,16},{1,65},{2,18},{3,67},{4,20},{5,69},{6,22},{7,71},{8,24},{9,... | collective-permute-start | bytes 792584 | tf_op jit(solution)/shard_map/ppermute | solution.py:47
  21.3 8.3 %collective-permute-start.8 = (bf16[1032,128]{1,0:T(8,128)(2,1)S(1)}, bf16[1032,128]{1,0:T(8,128)(2,1)S(1)}, u32[]{:S(2)}, u32[]{:S(2)}) collective-permute-start(bf16[1032,128]{1,0:T(8,128)(2,1)S(1)} %shard_map.146.refs_0_), channel_id=1, source_target_pairs={{0,8},{1,33},{2,10},{3,35},{4,12},{5,37},{6,14},{7,39},{8,0},{9,41... | collective-permute-start | bytes 792584 | tf_op jit(solution)/shard_map/ppermute | solution.py:47
  22.7 6.9 %collective-permute-start.9 = (bf16[1032,128]{1,0:T(8,128)(2,1)S(1)}, bf16[1032,128]{1,0:T(8,128)(2,1)S(1)}, u32[]{:S(2)}, u32[]{:S(2)}) collective-permute-start(bf16[1032,128]{1,0:T(8,128)(2,1)S(1)} %shard_map.146.refs_0_), channel_id=1, source_target_pairs={{0,24},{1,97},{2,26},{3,99},{4,28},{5,101},{6,30},{7,103},{8,16},{... | collective-permute-start | bytes 792584 | tf_op jit(solution)/shard_map/ppermute | solution.py:47
  29.6 19.1 %copy-start.4 = (f32[192]{0:T(256)S(1)}, f32[192]{0:T(256)}, u32[]{:S(2)}) copy-start(f32[192]{0:T(256)} %param.22) | copy-start | bytes 2308
  30.0 3.9 %collective-permute-start.10 = (bf16[64,1024]{1,0:T(8,128)(2,1)S(1)}, bf16[64,1024]{1,0:T(8,128)(2,1)S(1)}, u32[]{:S(2)}, u32[]{:S(2)}) collective-permute-start(bf16[64,1024]{1,0:T(8,128)(2,1)S(1)} %shard_map.147.refs_0_), channel_id=1, source_target_pairs={{0,32},{1,9},{2,34},{3,11},{4,36},{5,13},{6,38},{7,15},{8,40},{9,1... | collective-permute-start | bytes 393224 | tf_op jit(solution)/shard_map/ppermute | solution.py:47
  30.1 7.6 %collective-permute-start.11 = (bf16[64,1024]{1,0:T(8,128)(2,1)S(1)}, bf16[64,1024]{1,0:T(8,128)(2,1)S(1)}, u32[]{:S(2)}, u32[]{:S(2)}) collective-permute-start(bf16[64,1024]{1,0:T(8,128)(2,1)S(1)} %shard_map.147.refs_0_), channel_id=1, source_target_pairs={{0,64},{1,17},{2,66},{3,19},{4,68},{5,21},{6,70},{7,23},{8,72},{9,... | collective-permute-start | bytes 393224 | tf_op jit(solution)/shard_map/ppermute | solution.py:47
  33.9 5.2 %collective-permute-start.12 = (bf16[64,1024]{1,0:T(8,128)(2,1)S(1)}, bf16[64,1024]{1,0:T(8,128)(2,1)S(1)}, u32[]{:S(2)}, u32[]{:S(2)}) collective-permute-start(bf16[64,1024]{1,0:T(8,128)(2,1)S(1)} %shard_map.147.refs_0_), channel_id=1, source_target_pairs={{0,96},{1,25},{2,98},{3,27},{4,100},{5,29},{6,102},{7,31},{8,104},... | collective-permute-start | bytes 393224 | tf_op jit(solution)/shard_map/ppermute | solution.py:47
  39.1 13.3 %copy-start.2 = (f32[192,1024]{1,0:T(8,128)S(1)}, f32[192,1024]{1,0:T(8,128)}, u32[]{:S(2)}) copy-start(f32[192,1024]{1,0:T(8,128)} %refs_0_.1) | copy-start | bytes 2359300
  39.1 13.3 %copy-start.3 = (f32[192,1024]{1,0:T(8,128)S(1)}, f32[192,1024]{1,0:T(8,128)}, u32[]{:S(2)}) copy-start(f32[192,1024]{1,0:T(8,128)} %refs_2_.1) | copy-start | bytes 2359300
  39.6 5.5 %collective-permute-start.13 = (bf16[192,128]{1,0:T(8,128)(2,1)S(1)}, bf16[192,128]{1,0:T(8,128)(2,1)S(1)}, u32[]{:S(2)}, u32[]{:S(2)}) collective-permute-start(bf16[192,128]{1,0:T(8,128)(2,1)S(1)} %get-tuple-element.37), channel_id=1, source_target_pairs={{0,1},{1,0},{2,3},{3,2},{4,5},{5,4},{6,7},{7,6},{8,9},{9,8},{10,11... | collective-permute-start | bytes 147464 | tf_op jit(solution)/shard_map/ppermute | solution.py:51
  45.0 4.5 %collective-permute-start.14 = (bf16[192,128]{1,0:T(8,128)(2,1)S(1)}, bf16[192,128]{1,0:T(8,128)(2,1)S(1)}, u32[]{:S(2)}, u32[]{:S(2)}) collective-permute-start(bf16[192,128]{1,0:T(8,128)(2,1)S(1)} %fusion.1), channel_id=1, source_target_pairs={{0,4},{1,5},{2,6},{3,7},{4,0},{5,1},{6,2},{7,3},{8,12},{9,13},{10,... | collective-permute-start | bytes 147464 | tf_op jit(solution)/shard_map/ppermute | solution.py:57
  47.9 3.1 %collective-permute-start.15 = (bf16[192,128]{1,0:T(8,128)(2,1)S(1)}, bf16[192,128]{1,0:T(8,128)(2,1)S(1)}, u32[]{:S(2)}, u32[]{:S(2)}) collective-permute-start(bf16[192,128]{1,0:T(8,128)(2,1)S(1)} %fusion.1), channel_id=1, source_target_pairs={{0,2},{1,3},{2,0},{3,1},{4,6},{5,7},{6,4},{7,5},{8,10},{9,11},{10,... | collective-permute-start | bytes 147464 | tf_op jit(solution)/shard_map/ppermute | solution.py:57
  48.2 4.2 %collective-permute-start.16 = (bf16[192,128]{1,0:T(8,128)(2,1)S(1)}, bf16[192,128]{1,0:T(8,128)(2,1)S(1)}, u32[]{:S(2)}, u32[]{:S(2)}) collective-permute-start(bf16[192,128]{1,0:T(8,128)(2,1)S(1)} %fusion.1), channel_id=1, source_target_pairs={{0,6},{1,7},{2,4},{3,5},{4,2},{5,3},{6,0},{7,1},{8,14},{9,15},{10,... | collective-permute-start | bytes 147464 | tf_op jit(solution)/shard_map/ppermute | solution.py:57
  53.0 7.1 %collective-permute-start.17 = (bf16[1032,128]{1,0:T(8,128)(2,1)S(1)}, bf16[1032,128]{1,0:T(8,128)(2,1)S(1)}, u32[]{:S(2)}, u32[]{:S(2)}) collective-permute-start(bf16[1032,128]{1,0:T(8,128)(2,1)S(1)} %get-tuple-element.42), channel_id=1, source_target_pairs={{0,64},{1,17},{2,66},{3,19},{4,68},{5,21},{6,70},{7,23},{8,72},{9,... | collective-permute-start | bytes 792584 | tf_op jit(solution)/shard_map/ppermute | solution.py:47
  55.2 7.3 %collective-permute-start.18 = (bf16[1032,128]{1,0:T(8,128)(2,1)S(1)}, bf16[1032,128]{1,0:T(8,128)(2,1)S(1)}, u32[]{:S(2)}, u32[]{:S(2)}) collective-permute-start(bf16[1032,128]{1,0:T(8,128)(2,1)S(1)} %get-tuple-element.43), channel_id=1, source_target_pairs={{0,32},{1,9},{2,34},{3,11},{4,36},{5,13},{6,38},{7,15},{8,40},{9,1... | collective-permute-start | bytes 792584 | tf_op jit(solution)/shard_map/ppermute | solution.py:47
  55.6 7.3 %collective-permute-start.19 = (bf16[1032,128]{1,0:T(8,128)(2,1)S(1)}, bf16[1032,128]{1,0:T(8,128)(2,1)S(1)}, u32[]{:S(2)}, u32[]{:S(2)}) collective-permute-start(bf16[1032,128]{1,0:T(8,128)(2,1)S(1)} %get-tuple-element.44), channel_id=1, source_target_pairs={{0,96},{1,25},{2,98},{3,27},{4,100},{5,29},{6,102},{7,31},{8,104},... | collective-permute-start | bytes 792584 | tf_op jit(solution)/shard_map/ppermute | solution.py:47
  63.2 18.8 %copy-start.1 = (f32[1024,192]{0,1:T(8,128)S(1)}, f32[1024,192]{0,1:T(8,128)}, u32[]{:S(2)}) copy-start(f32[1024,192]{0,1:T(8,128)} %param.26) | copy-start | bytes 2359300
  63.2 6.9 %collective-permute-start.20 = (bf16[1032,128]{1,0:T(8,128)(2,1)S(1)}, bf16[1032,128]{1,0:T(8,128)(2,1)S(1)}, u32[]{:S(2)}, u32[]{:S(2)}) collective-permute-start(bf16[1032,128]{1,0:T(8,128)(2,1)S(1)} %shard_map.150.refs_0_), channel_id=1, source_target_pairs={{0,16},{1,65},{2,18},{3,67},{4,20},{5,69},{6,22},{7,71},{8,24},{9,... | collective-permute-start | bytes 792584 | tf_op jit(solution)/shard_map/ppermute | solution.py:47
  63.3 6.9 %collective-permute-start.21 = (bf16[1032,128]{1,0:T(8,128)(2,1)S(1)}, bf16[1032,128]{1,0:T(8,128)(2,1)S(1)}, u32[]{:S(2)}, u32[]{:S(2)}) collective-permute-start(bf16[1032,128]{1,0:T(8,128)(2,1)S(1)} %shard_map.150.refs_0_), channel_id=1, source_target_pairs={{0,8},{1,33},{2,10},{3,35},{4,12},{5,37},{6,14},{7,39},{8,0},{9,41... | collective-permute-start | bytes 792584 | tf_op jit(solution)/shard_map/ppermute | solution.py:47
  63.6 9.5 %collective-permute-start.22 = (bf16[1032,128]{1,0:T(8,128)(2,1)S(1)}, bf16[1032,128]{1,0:T(8,128)(2,1)S(1)}, u32[]{:S(2)}, u32[]{:S(2)}) collective-permute-start(bf16[1032,128]{1,0:T(8,128)(2,1)S(1)} %shard_map.150.refs_0_), channel_id=1, source_target_pairs={{0,24},{1,97},{2,26},{3,99},{4,28},{5,101},{6,30},{7,103},{8,16},{... | collective-permute-start | bytes 792584 | tf_op jit(solution)/shard_map/ppermute | solution.py:47
  73.6 12.2 %copy-start.5 = (f32[192]{0:T(256)S(1)}, f32[192]{0:T(256)}, u32[]{:S(2)}) copy-start(f32[192]{0:T(256)} %param.29) | copy-start | bytes 2308
  73.6 3.9 %collective-permute-start.23 = (bf16[32,2048]{1,0:T(8,128)(2,1)S(1)}, bf16[32,2048]{1,0:T(8,128)(2,1)S(1)}, u32[]{:S(2)}, u32[]{:S(2)}) collective-permute-start(bf16[32,2048]{1,0:T(8,128)(2,1)S(1)} %shard_map.151.refs_0_), channel_id=1, source_target_pairs={{0,32},{1,9},{2,34},{3,11},{4,36},{5,13},{6,38},{7,15},{8,40},{9,1... | collective-permute-start | bytes 393224 | tf_op jit(solution)/shard_map/ppermute | solution.py:47
  74.7 5.9 %collective-permute-start.24 = (bf16[32,2048]{1,0:T(8,128)(2,1)S(1)}, bf16[32,2048]{1,0:T(8,128)(2,1)S(1)}, u32[]{:S(2)}, u32[]{:S(2)}) collective-permute-start(bf16[32,2048]{1,0:T(8,128)(2,1)S(1)} %shard_map.151.refs_0_), channel_id=1, source_target_pairs={{0,64},{1,17},{2,66},{3,19},{4,68},{5,21},{6,70},{7,23},{8,72},{9,... | collective-permute-start | bytes 393224 | tf_op jit(solution)/shard_map/ppermute | solution.py:47
  76.8 5.2 %collective-permute-start.25 = (bf16[32,2048]{1,0:T(8,128)(2,1)S(1)}, bf16[32,2048]{1,0:T(8,128)(2,1)S(1)}, u32[]{:S(2)}, u32[]{:S(2)}) collective-permute-start(bf16[32,2048]{1,0:T(8,128)(2,1)S(1)} %shard_map.151.refs_0_), channel_id=1, source_target_pairs={{0,96},{1,25},{2,98},{3,27},{4,100},{5,29},{6,102},{7,31},{8,104},... | collective-permute-start | bytes 393224 | tf_op jit(solution)/shard_map/ppermute | solution.py:47
  82.4 4.5 %collective-permute-start.26 = (bf16[192,128]{1,0:T(8,128)(2,1)S(1)}, bf16[192,128]{1,0:T(8,128)(2,1)S(1)}, u32[]{:S(2)}, u32[]{:S(2)}) collective-permute-start(bf16[192,128]{1,0:T(8,128)(2,1)S(1)} %shard_map.152), channel_id=1, source_target_pairs={{0,4},{1,5},{2,6},{3,7},{4,0},{5,1},{6,2},{7,3},{8,12},{9,13},{10,... | collective-permute-start | bytes 147464 | tf_op jit(solution)/shard_map/ppermute | solution.py:57
  83.9 3.1 %collective-permute-start.27 = (bf16[192,128]{1,0:T(8,128)(2,1)S(1)}, bf16[192,128]{1,0:T(8,128)(2,1)S(1)}, u32[]{:S(2)}, u32[]{:S(2)}) collective-permute-start(bf16[192,128]{1,0:T(8,128)(2,1)S(1)} %shard_map.152), channel_id=1, source_target_pairs={{0,2},{1,3},{2,0},{3,1},{4,6},{5,7},{6,4},{7,5},{8,10},{9,11},{10,... | collective-permute-start | bytes 147464 | tf_op jit(solution)/shard_map/ppermute | solution.py:57
  84.4 4.2 %collective-permute-start.28 = (bf16[192,128]{1,0:T(8,128)(2,1)S(1)}, bf16[192,128]{1,0:T(8,128)(2,1)S(1)}, u32[]{:S(2)}, u32[]{:S(2)}) collective-permute-start(bf16[192,128]{1,0:T(8,128)(2,1)S(1)} %shard_map.152), channel_id=1, source_target_pairs={{0,6},{1,7},{2,4},{3,5},{4,2},{5,3},{6,0},{7,1},{8,14},{9,15},{10,... | collective-permute-start | bytes 147464 | tf_op jit(solution)/shard_map/ppermute | solution.py:57
  88.7 5.6 %collective-permute-start.29 = (bf16[192,128]{1,0:T(8,128)(2,1)S(1)}, bf16[192,128]{1,0:T(8,128)(2,1)S(1)}, u32[]{:S(2)}, u32[]{:S(2)}) collective-permute-start(bf16[192,128]{1,0:T(8,128)(2,1)S(1)} %add_convert_fusion), channel_id=1, source_target_pairs={{0,1},{1,0},{2,3},{3,2},{4,5},{5,4},{6,7},{7,6},{8,9},{9,8},{10,11... | collective-permute-start | bytes 147464 | tf_op jit(solution)/shard_map/ppermute | solution.py:51
where the time goes:
time: 95.1 us; the launch traced here: 95 us
  starting transfers between devices  45.7 us (48%)
  waiting for transfers between devices  43.5 us (46%)
  Pallas kernels  4.7 us (5%)
    ppermute x18, waiting for transfers between devices, swapped(): return lax.ppermute(x, ('ra', 'cb'), pairs_of(k, along_f))  34.5 us
    ppermute x18, starting transfers between devices, swapped(): return lax.ppermute(x, ('ra', 'cb'), pairs_of(k, along_f))  26.5 us
    ppermute x6, starting transfers between devices, other_core(): lax.ppermute(x, 'cb', [(i, i ^ 1) for i in range(lax.axis_size('cb'))])  12.2 us
    ppermute x6, starting transfers between devices, sum_over_x(): lax.ppermute(sent, 'cb', [(i, i ^ 2 * k) for i in range(n)]).astype(F32)  7.02 us
    ppermute x6, waiting for transfers between devices, sum_over_x(): lax.ppermute(sent, 'cb', [(i, i ^ 2 * k) for i in range(n)]).astype(F32)  6.41 us
    ppermute x6, waiting for transfers between devices, other_core(): lax.ppermute(x, 'cb', [(i, i ^ 1) for i in range(lax.axis_size('cb'))])  2.6 us
    pallas_call x2, Pallas kernels, products(): pl.pallas_call(fetching_kernel if small else products_kernel, out_shape=o...  2.5 us
    pallas_call x6, Pallas kernels, call(): pl.pallas_call(kernel, out_shape=[jax.ShapeDtypeStruct(shape, BF16) for s...  2.2 us
  transfers between devices with their start and end apart: 30, of which 23 were waited for; matrix products, arithmetic and copies ran while one was open for 0% of the time, Pallas kernels for 2%

commit v1 on v0

--- a/solution.py
+++ b/solution.py
@@ -12,8 +12,9 @@
 SIDE = 4
 WIDE = 1024
 PIECE = 96
-ORDER = (2, 1, 3)
-X_ORDER = (2, 1, 3)
+ORDER = (2, 3, 1)
+X_ORDER = (2, 3, 1)
+G_ORDER = (2, 3, 1)
 BF16 = jnp.bfloat16
 F32 = jnp.float32
 VMEM = pl.BlockSpec(memory_space=pltpu.VMEM)
@@ -263,7 +264,7 @@
     rows = mine.shape[0] // (2 * units // 128)
     kernel = functools.partial(hidden_kernel, len(scales))
     (hidden,) = call(kernel, [(rows, units)], mine, *peers, *scales)
-    others = {k: swapped(hidden, k, True) for k in ORDER}
+    others = {k: swapped(hidden, k, True) for k in G_ORDER}
     return hidden, others[1], others[2], others[3]
 
 

time: 95.1 us -> 93.3 us (0.981)
  starting transfers between devices: 45.7 us -> 43.4 us
    ppermute x18, starting transfers between devices: 26.5 us -> 25 us  [swapped(): return lax.ppermute(x, ('ra', 'cb'), pairs_of(k, along_f))]
  transfers between devices with their start and end apart: 30 -> 30, of which waited for: 23 -> 22; matrix products, arithmetic and copies ran while one was open for 0% -> 0% of each run, Pallas kernels for 2% -> 2%
where the time goes in v1:
time: 93.3 us; the launch traced here: 93.2 us
  waiting for transfers between devices  44 us (47%)
  starting transfers between devices  43.4 us (47%)
  Pallas kernels  4.7 us (5%)
    ppermute x18, waiting for transfers between devices, swapped(): return lax.ppermute(x, ('ra', 'cb'), pairs_of(k, along_f))  35 us
    ppermute x18, starting transfers between devices, swapped(): return lax.ppermute(x, ('ra', 'cb'), pairs_of(k, along_f))  25 us
    ppermute x6, starting transfers between devices, other_core(): lax.ppermute(x, 'cb', [(i, i ^ 1) for i in range(lax.axis_size('cb'))])  11.4 us
    ppermute x6, starting transfers between devices, sum_over_x(): lax.ppermute(sent, 'cb', [(i, i ^ 2 * k) for i in range(n)]).astype(F32)  7.02 us
    ppermute x6, waiting for transfers between devices, sum_over_x(): lax.ppermute(sent, 'cb', [(i, i ^ 2 * k) for i in range(n)]).astype(F32)  6.41 us
    ppermute x6, waiting for transfers between devices, other_core(): lax.ppermute(x, 'cb', [(i, i ^ 1) for i in range(lax.axis_size('cb'))])  2.6 us
    pallas_call x2, Pallas kernels, products(): pl.pallas_call(fetching_kernel if small else products_kernel, out_shape=o...  2.5 us
    pallas_call x6, Pallas kernels, call(): pl.pallas_call(kernel, out_shape=[jax.ShapeDtypeStruct(shape, BF16) for s...  2.2 us
  transfers between devices with their start and end apart: 30, of which 22 were waited for; matrix products, arithmetic and copies ran while one was open for 0% of the time, Pallas kernels for 2%

profile of v1, /device:TPU:1, one launch (start us, length us, event | category | flops | bytes accessed | tf_op | source)
XLA Modules:
  0.0 93.2 jit_solution(1911091916772310123)
XLA Ops:
  0.0 1.4 %collective-permute-start.5 = (f32[192,1024]{1,0:T(8,128)}, f32[192,1024]{1,0:T(8,128)S(1)}, u32[]{:S(2)}, u32[]{:S(2)}) collective-permute-start(f32[192,1024]{1,0:T(8,128)} %bitcast.12), channel_id=1, source_target_pairs={{0,1},{1,0},{2,3},{3,2},{4,5},{5,4},{6,7},{7,6},{8,9},{9,8},{10,11... | collective-permute-start | bytes 2359304 | tf_op jit(solution)/shard_map/ppermute | solution.py:52
  1.4 0.5 collective-permute-start.4
  1.9 2.0 %shard_map.145 = (bf16[1032,128]{1,0:T(8,128)(2,1)S(1)}, bf16[1032,128]{1,0:T(8,128)(2,1)S(1)}, bf16[1032,128]{1,0:T(8,128)(2,1)S(1)}, bf16[1032,128]{1,0:T(8,12...) custom-call(bf16[192,256]{1,0:T(8,128)(2,1)} %bitcast.14, ...), custom_call_target="tpu_custom_call" | custom-call | flops 201326592 | bytes 1572864 | tf_op jit(solution)/shard_map/pallas_call | solution.py:177
  3.9 3.1 %collective-permute-start = (bf16[1032,128]{1,0:T(8,128)(2,1)S(1)}, bf16[1032,128]{1,0:T(8,128)(2,1)S(1)}, u32[]{:S(2)}, u32[]{:S(2)}) collective-permute-start(bf16[1032,128]{1,0:T(8,128)(2,1)S(1)} %get-tuple-element.28), channel_id=1, source_target_pairs={{0,64},{1,17},{2,66},{3,19},{4,68},{5,21},{6,70},{7,23},{8,72},{9,... | collective-permute-start | bytes 792584 | tf_op jit(solution)/shard_map/ppermute | solution.py:48
  7.0 1.0 %collective-permute-start.6 = (f32[2,1,1024]{2,1,0:T(1,128)S(1)}, f32[2,1,1024]{2,1,0:T(1,128)S(1)}, u32[]{:S(2)}, u32[]{:S(2)}) collective-permute-start(f32[2,1,1024]{2,1,0:T(1,128)S(1)} %get-tuple-element.31.refs_4_), channel_id=1, source_target_pairs={{0,1},{1,0},{2,3},{3,2},{4,5},{5,4},{6,7},{7,6},{8,9},{9,8},{10,11... | collective-permute-start | bytes 24584 | tf_op jit(solution)/shard_map/ppermute | solution.py:52
  8.0 0.8 collective-permute-done.6.refs_5_
  8.8 2.7 %collective-permute-start.1 = (bf16[1032,128]{1,0:T(8,128)(2,1)S(1)}, bf16[1032,128]{1,0:T(8,128)(2,1)S(1)}, u32[]{:S(2)}, u32[]{:S(2)}) collective-permute-start(bf16[1032,128]{1,0:T(8,128)(2,1)S(1)} %get-tuple-element.29), channel_id=1, source_target_pairs={{0,96},{1,25},{2,98},{3,27},{4,100},{5,29},{6,102},{7,31},{8,104},... | collective-permute-start | bytes 792584 | tf_op jit(solution)/shard_map/ppermute | solution.py:48
  11.5 0.9 collective-permute-start.2
  12.4 3.2 %collective-permute-done.1.refs_2_ = bf16[1032,128]{1,0:T(8,128)(2,1)S(1)} collective-permute-done((bf16[1032,128]{1,0:T(8,128)(2,1)S(1)}, bf16[1032,128]{1,0:T(8,128)(2,1)S(1)}, u32[]{:S(2)}, u32[]{:S(2)}) %collective-permute-start.1) | collective-permute-done | bytes 264224 | tf_op jit(solution)/shard_map/ppermute | solution.py:48
  15.6 1.5 %collective-permute-done.2.refs_3_ = bf16[1032,128]{1,0:T(8,128)(2,1)S(1)} collective-permute-done((bf16[1032,128]{1,0:T(8,128)(2,1)S(1)}, bf16[1032,128]{1,0:T(8,128)(2,1)S(1)}, u32[]{:S(2)}, u32[]{:S(2)}) %collective-permute-start.2) | collective-permute-done | bytes 264224 | tf_op jit(solution)/shard_map/ppermute | solution.py:48
  17.1 0.3 shard_map.146.refs_0_
  17.4 0.0 copy-start
  17.4 3.1 %collective-permute-start.7 = (bf16[1032,128]{1,0:T(8,128)(2,1)S(1)}, bf16[1032,128]{1,0:T(8,128)(2,1)S(1)}, u32[]{:S(2)}, u32[]{:S(2)}) collective-permute-start(bf16[1032,128]{1,0:T(8,128)(2,1)S(1)} %shard_map.146.refs_0_), channel_id=1, source_target_pairs={{0,16},{1,65},{2,18},{3,67},{4,20},{5,69},{6,22},{7,71},{8,24},{9,... | collective-permute-start | bytes 792584 | tf_op jit(solution)/shard_map/ppermute | solution.py:48
  20.5 0.4 collective-permute-start.8
  20.9 0.5 collective-permute-start.9
  21.4 3.2 %collective-permute-done.7.refs_1_ = bf16[1032,128]{1,0:T(8,128)(2,1)S(1)} collective-permute-done((bf16[1032,128]{1,0:T(8,128)(2,1)S(1)}, bf16[1032,128]{1,0:T(8,128)(2,1)S(1)}, u32[]{:S(2)}, u32[]{:S(2)}) %collective-permute-start.7) | collective-permute-done | bytes 264224 | tf_op jit(solution)/shard_map/ppermute | solution.py:48
  24.6 2.8 %collective-permute-done.8.refs_2_ = bf16[1032,128]{1,0:T(8,128)(2,1)S(1)} collective-permute-done((bf16[1032,128]{1,0:T(8,128)(2,1)S(1)}, bf16[1032,128]{1,0:T(8,128)(2,1)S(1)}, u32[]{:S(2)}, u32[]{:S(2)}) %collective-permute-start.8) | collective-permute-done | bytes 264224 | tf_op jit(solution)/shard_map/ppermute | solution.py:48
  27.4 0.9 %collective-permute-done.9.refs_3_ = bf16[1032,128]{1,0:T(8,128)(2,1)S(1)} collective-permute-done((bf16[1032,128]{1,0:T(8,128)(2,1)S(1)}, bf16[1032,128]{1,0:T(8,128)(2,1)S(1)}, u32[]{:S(2)}, u32[]{:S(2)}) %collective-permute-start.9) | collective-permute-done | bytes 264224 | tf_op jit(solution)/shard_map/ppermute | solution.py:48
  28.3 0.4 shard_map.147.refs_0_
  28.7 1.4 %collective-permute-start.10 = (bf16[64,1024]{1,0:T(8,128)(2,1)S(1)}, bf16[64,1024]{1,0:T(8,128)(2,1)S(1)}, u32[]{:S(2)}, u32[]{:S(2)}) collective-permute-start(bf16[64,1024]{1,0:T(8,128)(2,1)S(1)} %shard_map.147.refs_0_), channel_id=1, source_target_pairs={{0,32},{1,9},{2,34},{3,11},{4,36},{5,13},{6,38},{7,15},{8,40},{9,1... | collective-permute-start | bytes 393224 | tf_op jit(solution)/shard_map/ppermute | solution.py:48
  30.1 2.6 %collective-permute-start.11 = (bf16[64,1024]{1,0:T(8,128)(2,1)S(1)}, bf16[64,1024]{1,0:T(8,128)(2,1)S(1)}, u32[]{:S(2)}, u32[]{:S(2)}) collective-permute-start(bf16[64,1024]{1,0:T(8,128)(2,1)S(1)} %shard_map.147.refs_0_), channel_id=1, source_target_pairs={{0,64},{1,17},{2,66},{3,19},{4,68},{5,21},{6,70},{7,23},{8,72},{9,... | collective-permute-start | bytes 393224 | tf_op jit(solution)/shard_map/ppermute | solution.py:48
  32.7 3.8 %collective-permute-done.11.refs_2_ = bf16[64,1024]{1,0:T(8,128)(2,1)S(1)} collective-permute-done((bf16[64,1024]{1,0:T(8,128)(2,1)S(1)}, bf16[64,1024]{1,0:T(8,128)(2,1)S(1)}, u32[]{:S(2)}, u32[]{:S(2)}) %collective-permute-start.11) | collective-permute-done | bytes 131104 | tf_op jit(solution)/shard_map/ppermute | solution.py:48
  36.5 1.4 %collective-permute-done.12.refs_3_ = bf16[64,1024]{1,0:T(8,128)(2,1)S(1)} collective-permute-done((bf16[64,1024]{1,0:T(8,128)(2,1)S(1)}, bf16[64,1024]{1,0:T(8,128)(2,1)S(1)}, u32[]{:S(2)}, u32[]{:S(2)}) %collective-permute-start.12) | collective-permute-done | bytes 131104 | tf_op jit(solution)/shard_map/ppermute | solution.py:48
  37.9 0.4 shard_map.148
  38.3 4.3 %collective-permute-start.13 = (bf16[192,128]{1,0:T(8,128)(2,1)S(1)}, bf16[192,128]{1,0:T(8,128)(2,1)S(1)}, u32[]{:S(2)}, u32[]{:S(2)}) collective-permute-start(bf16[192,128]{1,0:T(8,128)(2,1)S(1)} %get-tuple-element.37), channel_id=1, source_target_pairs={{0,1},{1,0},{2,3},{3,2},{4,5},{5,4},{6,7},{7,6},{8,9},{9,8},{10,11... | collective-permute-start | bytes 147464 | tf_op jit(solution)/shard_map/ppermute | solution.py:52
  42.6 0.9 collective-permute-done.13
  43.5 2.8 %collective-permute-start.14 = (bf16[192,128]{1,0:T(8,128)(2,1)S(1)}, bf16[192,128]{1,0:T(8,128)(2,1)S(1)}, u32[]{:S(2)}, u32[]{:S(2)}) collective-permute-start(bf16[192,128]{1,0:T(8,128)(2,1)S(1)} %fusion.1), channel_id=1, source_target_pairs={{0,4},{1,5},{2,6},{3,7},{4,0},{5,1},{6,2},{7,3},{8,12},{9,13},{10,... | collective-permute-start | bytes 147464 | tf_op jit(solution)/shard_map/ppermute | solution.py:58
  46.4 0.3 collective-permute-start.15
  46.7 0.5 collective-permute-start.16
  47.2 0.8 collective-permute-done.14
  48.1 1.4 %collective-permute-done.15 = bf16[192,128]{1,0:T(8,128)(2,1)S(1)} collective-permute-done((bf16[192,128]{1,0:T(8,128)(2,1)S(1)}, bf16[192,128]{1,0:T(8,128)(2,1)S(1)}, u32[]{:S(2)}, u32[]{:S(2)}) %collective-permute-start.15) | collective-permute-done | bytes 49184 | tf_op jit(solution)/shard_map/ppermute | solution.py:58
  49.5 1.3 %collective-permute-done.16 = bf16[192,128]{1,0:T(8,128)(2,1)S(1)} collective-permute-done((bf16[192,128]{1,0:T(8,128)(2,1)S(1)}, bf16[192,128]{1,0:T(8,128)(2,1)S(1)}, u32[]{:S(2)}, u32[]{:S(2)}) %collective-permute-start.16) | collective-permute-done | bytes 49184 | tf_op jit(solution)/shard_map/ppermute | solution.py:58
  50.8 0.1 add_convert_fusion.1.stream_ref
  51.0 0.5 shard_map.149
  51.5 1.8 %collective-permute-start.17 = (bf16[1032,128]{1,0:T(8,128)(2,1)S(1)}, bf16[1032,128]{1,0:T(8,128)(2,1)S(1)}, u32[]{:S(2)}, u32[]{:S(2)}) collective-permute-start(bf16[1032,128]{1,0:T(8,128)(2,1)S(1)} %get-tuple-element.42), channel_id=1, source_target_pairs={{0,64},{1,17},{2,66},{3,19},{4,68},{5,21},{6,70},{7,23},{8,72},{9,... | collective-permute-start | bytes 792584 | tf_op jit(solution)/shard_map/ppermute | solution.py:48
  53.3 1.7 %collective-permute-start.18 = (bf16[1032,128]{1,0:T(8,128)(2,1)S(1)}, bf16[1032,128]{1,0:T(8,128)(2,1)S(1)}, u32[]{:S(2)}, u32[]{:S(2)}) collective-permute-start(bf16[1032,128]{1,0:T(8,128)(2,1)S(1)} %get-tuple-element.43), channel_id=1, source_target_pairs={{0,96},{1,25},{2,98},{3,27},{4,100},{5,29},{6,102},{7,31},{8,104},... | collective-permute-start | bytes 792584 | tf_op jit(solution)/shard_map/ppermute | solution.py:48
  55.0 3.6 %collective-permute-done.17.refs_1_ = bf16[1032,128]{1,0:T(8,128)(2,1)S(1)} collective-permute-done((bf16[1032,128]{1,0:T(8,128)(2,1)S(1)}, bf16[1032,128]{1,0:T(8,128)(2,1)S(1)}, u32[]{:S(2)}, u32[]{:S(2)}) %collective-permute-start.17) | collective-permute-done | bytes 264224 | tf_op jit(solution)/shard_map/ppermute | solution.py:48
  58.6 2.8 %collective-permute-done.18.refs_2_ = bf16[1032,128]{1,0:T(8,128)(2,1)S(1)} collective-permute-done((bf16[1032,128]{1,0:T(8,128)(2,1)S(1)}, bf16[1032,128]{1,0:T(8,128)(2,1)S(1)}, u32[]{:S(2)}, u32[]{:S(2)}) %collective-permute-start.18) | collective-permute-done | bytes 264224 | tf_op jit(solution)/shard_map/ppermute | solution.py:48
  61.4 0.0 collective-permute-done.19.refs_3_
  61.4 0.3 shard_map.150.refs_0_
  61.7 0.0 copy-start.1
  61.7 0.1 collective-permute-start.20
  61.9 1.5 %collective-permute-start.21 = (bf16[1032,128]{1,0:T(8,128)(2,1)S(1)}, bf16[1032,128]{1,0:T(8,128)(2,1)S(1)}, u32[]{:S(2)}, u32[]{:S(2)}) collective-permute-start(bf16[1032,128]{1,0:T(8,128)(2,1)S(1)} %shard_map.150.refs_0_), channel_id=1, source_target_pairs={{0,24},{1,97},{2,26},{3,99},{4,28},{5,101},{6,30},{7,103},{8,16},{... | collective-permute-start | bytes 792584 | tf_op jit(solution)/shard_map/ppermute | solution.py:48
  63.3 1.2 %collective-permute-start.22 = (bf16[1032,128]{1,0:T(8,128)(2,1)S(1)}, bf16[1032,128]{1,0:T(8,128)(2,1)S(1)}, u32[]{:S(2)}, u32[]{:S(2)}) collective-permute-start(bf16[1032,128]{1,0:T(8,128)(2,1)S(1)} %shard_map.150.refs_0_), channel_id=1, source_target_pairs={{0,8},{1,33},{2,10},{3,35},{4,12},{5,37},{6,14},{7,39},{8,0},{9,41... | collective-permute-start | bytes 792584 | tf_op jit(solution)/shard_map/ppermute | solution.py:48
  64.5 4.2 %collective-permute-done.20.refs_1_ = bf16[1032,128]{1,0:T(8,128)(2,1)S(1)} collective-permute-done((bf16[1032,128]{1,0:T(8,128)(2,1)S(1)}, bf16[1032,128]{1,0:T(8,128)(2,1)S(1)}, u32[]{:S(2)}, u32[]{:S(2)}) %collective-permute-start.20) | collective-permute-done | bytes 264224 | tf_op jit(solution)/shard_map/ppermute | solution.py:48
  68.7 2.8 %collective-permute-done.21.refs_2_ = bf16[1032,128]{1,0:T(8,128)(2,1)S(1)} collective-permute-done((bf16[1032,128]{1,0:T(8,128)(2,1)S(1)}, bf16[1032,128]{1,0:T(8,128)(2,1)S(1)}, u32[]{:S(2)}, u32[]{:S(2)}) %collective-permute-start.21) | collective-permute-done | bytes 264224 | tf_op jit(solution)/shard_map/ppermute | solution.py:48
  71.5 0.4 shard_map.151.refs_0_
  71.9 0.0 copy-start.5
  71.9 1.0 %collective-permute-start.23 = (bf16[32,2048]{1,0:T(8,128)(2,1)S(1)}, bf16[32,2048]{1,0:T(8,128)(2,1)S(1)}, u32[]{:S(2)}, u32[]{:S(2)}) collective-permute-start(bf16[32,2048]{1,0:T(8,128)(2,1)S(1)} %shard_map.151.refs_0_), channel_id=1, source_target_pairs={{0,32},{1,9},{2,34},{3,11},{4,36},{5,13},{6,38},{7,15},{8,40},{9,1... | collective-permute-start | bytes 393224 | tf_op jit(solution)/shard_map/ppermute | solution.py:48
  72.9 2.6 %collective-permute-start.24 = (bf16[32,2048]{1,0:T(8,128)(2,1)S(1)}, bf16[32,2048]{1,0:T(8,128)(2,1)S(1)}, u32[]{:S(2)}, u32[]{:S(2)}) collective-permute-start(bf16[32,2048]{1,0:T(8,128)(2,1)S(1)} %shard_map.151.refs_0_), channel_id=1, source_target_pairs={{0,64},{1,17},{2,66},{3,19},{4,68},{5,21},{6,70},{7,23},{8,72},{9,... | collective-permute-start | bytes 393224 | tf_op jit(solution)/shard_map/ppermute | solution.py:48
  75.5 0.3 collective-permute-start.25
  75.8 0.3 collective-permute-done.23.refs_1_
  76.2 3.1 %collective-permute-done.24.refs_2_ = bf16[32,2048]{1,0:T(8,128)(2,1)S(1)} collective-permute-done((bf16[32,2048]{1,0:T(8,128)(2,1)S(1)}, bf16[32,2048]{1,0:T(8,128)(2,1)S(1)}, u32[]{:S(2)}, u32[]{:S(2)}) %collective-permute-start.24) | collective-permute-done | bytes 131104 | tf_op jit(solution)/shard_map/ppermute | solution.py:48
  79.3 1.4 %collective-permute-done.25.refs_3_ = bf16[32,2048]{1,0:T(8,128)(2,1)S(1)} collective-permute-done((bf16[32,2048]{1,0:T(8,128)(2,1)S(1)}, bf16[32,2048]{1,0:T(8,128)(2,1)S(1)}, u32[]{:S(2)}, u32[]{:S(2)}) %collective-permute-start.25) | collective-permute-done | bytes 131104 | tf_op jit(solution)/shard_map/ppermute | solution.py:48
  80.7 0.4 shard_map.152
  81.1 1.4 %collective-permute-start.26 = (bf16[192,128]{1,0:T(8,128)(2,1)S(1)}, bf16[192,128]{1,0:T(8,128)(2,1)S(1)}, u32[]{:S(2)}, u32[]{:S(2)}) collective-permute-start(bf16[192,128]{1,0:T(8,128)(2,1)S(1)} %shard_map.152), channel_id=1, source_target_pairs={{0,4},{1,5},{2,6},{3,7},{4,0},{5,1},{6,2},{7,3},{8,12},{9,13},{10,... | collective-permute-start | bytes 147464 | tf_op jit(solution)/shard_map/ppermute | solution.py:58
  82.6 0.6 collective-permute-start.27
  83.1 1.3 %collective-permute-start.28 = (bf16[192,128]{1,0:T(8,128)(2,1)S(1)}, bf16[192,128]{1,0:T(8,128)(2,1)S(1)}, u32[]{:S(2)}, u32[]{:S(2)}) collective-permute-start(bf16[192,128]{1,0:T(8,128)(2,1)S(1)} %shard_map.152), channel_id=1, source_target_pairs={{0,6},{1,7},{2,4},{3,5},{4,2},{5,3},{6,0},{7,1},{8,14},{9,15},{10,... | collective-permute-start | bytes 147464 | tf_op jit(solution)/shard_map/ppermute | solution.py:58
  84.5 1.2 %collective-permute-done.26 = bf16[192,128]{1,0:T(8,128)(2,1)S(1)} collective-permute-done((bf16[192,128]{1,0:T(8,128)(2,1)S(1)}, bf16[192,128]{1,0:T(8,128)(2,1)S(1)}, u32[]{:S(2)}, u32[]{:S(2)}) %collective-permute-start.26) | collective-permute-done | bytes 49184 | tf_op jit(solution)/shard_map/ppermute | solution.py:58
  85.7 1.6 %collective-permute-done.28 = bf16[192,128]{1,0:T(8,128)(2,1)S(1)} collective-permute-done((bf16[192,128]{1,0:T(8,128)(2,1)S(1)}, bf16[192,128]{1,0:T(8,128)(2,1)S(1)}, u32[]{:S(2)}, u32[]{:S(2)}) %collective-permute-start.28) | collective-permute-done | bytes 49184 | tf_op jit(solution)/shard_map/ppermute | solution.py:58
  87.3 0.1 add_convert_fusion
  87.4 4.3 %collective-permute-start.29 = (bf16[192,128]{1,0:T(8,128)(2,1)S(1)}, bf16[192,128]{1,0:T(8,128)(2,1)S(1)}, u32[]{:S(2)}, u32[]{:S(2)}) collective-permute-start(bf16[192,128]{1,0:T(8,128)(2,1)S(1)} %add_convert_fusion), channel_id=1, source_target_pairs={{0,1},{1,0},{2,3},{3,2},{4,5},{5,4},{6,7},{7,6},{8,9},{9,8},{10,11... | collective-permute-start | bytes 147464 | tf_op jit(solution)/shard_map/ppermute | solution.py:52
  91.6 0.9 collective-permute-done.29
  92.5 0.7 fusion
  (22 shorter events, 0.1 us)
Async XLA Ops:
  0.0 17.1 %collective-permute-start.5 = (f32[192,1024]{1,0:T(8,128)}, f32[192,1024]{1,0:T(8,128)S(1)}, u32[]{:S(2)}, u32[]{:S(2)}) collective-permute-start(f32[192,1024]{1,0:T(8,128)} %bitcast.12), channel_id=1, source_target_pairs={{0,1},{1,0},{2,3},{3,2},{4,5},{5,4},{6,7},{7,6},{8,9},{9,8},{10,11... | collective-permute-start | bytes 2359304 | tf_op jit(solution)/shard_map/ppermute | solution.py:52
  1.4 15.7 %collective-permute-start.3 = (f32[192,1024]{1,0:T(8,128)}, f32[192,1024]{1,0:T(8,128)S(1)}, u32[]{:S(2)}, u32[]{:S(2)}) collective-permute-start(f32[192,1024]{1,0:T(8,128)} %refs_0_.1), channel_id=1, source_target_pairs={{0,1},{1,0},{2,3},{3,2},{4,5},{5,4},{6,7},{7,6},{8,9},{9,8},{10,11... | collective-permute-start | bytes 2359304 | tf_op jit(solution)/shard_map/ppermute | solution.py:52
  1.4 15.7 %collective-permute-start.4 = (f32[192,1024]{1,0:T(8,128)}, f32[192,1024]{1,0:T(8,128)S(1)}, u32[]{:S(2)}, u32[]{:S(2)}) collective-permute-start(f32[192,1024]{1,0:T(8,128)} %refs_2_.1), channel_id=1, source_target_pairs={{0,1},{1,0},{2,3},{3,2},{4,5},{5,4},{6,7},{7,6},{8,9},{9,8},{10,11... | collective-permute-start | bytes 2359304 | tf_op jit(solution)/shard_map/ppermute | solution.py:52
  3.9 7.6 %collective-permute-start = (bf16[1032,128]{1,0:T(8,128)(2,1)S(1)}, bf16[1032,128]{1,0:T(8,128)(2,1)S(1)}, u32[]{:S(2)}, u32[]{:S(2)}) collective-permute-start(bf16[1032,128]{1,0:T(8,128)(2,1)S(1)} %get-tuple-element.28), channel_id=1, source_target_pairs={{0,64},{1,17},{2,66},{3,19},{4,68},{5,21},{6,70},{7,23},{8,72},{9,... | collective-permute-start | bytes 792584 | tf_op jit(solution)/shard_map/ppermute | solution.py:48
  7.0 1.8 %collective-permute-start.6 = (f32[2,1,1024]{2,1,0:T(1,128)S(1)}, f32[2,1,1024]{2,1,0:T(1,128)S(1)}, u32[]{:S(2)}, u32[]{:S(2)}) collective-permute-start(f32[2,1,1024]{2,1,0:T(1,128)S(1)} %get-tuple-element.31.refs_4_), channel_id=1, source_target_pairs={{0,1},{1,0},{2,3},{3,2},{4,5},{5,4},{6,7},{7,6},{8,9},{9,8},{10,11... | collective-permute-start | bytes 24584 | tf_op jit(solution)/shard_map/ppermute | solution.py:52
  8.8 6.8 %collective-permute-start.1 = (bf16[1032,128]{1,0:T(8,128)(2,1)S(1)}, bf16[1032,128]{1,0:T(8,128)(2,1)S(1)}, u32[]{:S(2)}, u32[]{:S(2)}) collective-permute-start(bf16[1032,128]{1,0:T(8,128)(2,1)S(1)} %get-tuple-element.29), channel_id=1, source_target_pairs={{0,96},{1,25},{2,98},{3,27},{4,100},{5,29},{6,102},{7,31},{8,104},... | collective-permute-start | bytes 792584 | tf_op jit(solution)/shard_map/ppermute | solution.py:48
  11.5 5.5 %collective-permute-start.2 = (bf16[1032,128]{1,0:T(8,128)(2,1)S(1)}, bf16[1032,128]{1,0:T(8,128)(2,1)S(1)}, u32[]{:S(2)}, u32[]{:S(2)}) collective-permute-start(bf16[1032,128]{1,0:T(8,128)(2,1)S(1)} %get-tuple-element.30), channel_id=1, source_target_pairs={{0,32},{1,9},{2,34},{3,11},{4,36},{5,13},{6,38},{7,15},{8,40},{9,1... | collective-permute-start | bytes 792584 | tf_op jit(solution)/shard_map/ppermute | solution.py:48
  17.4 20.5 %copy-start = (f32[1024,192]{0,1:T(8,128)S(1)}, f32[1024,192]{0,1:T(8,128)}, u32[]{:S(2)}) copy-start(f32[1024,192]{0,1:T(8,128)} %param.19) | copy-start | bytes 2359300
  17.4 7.2 %collective-permute-start.7 = (bf16[1032,128]{1,0:T(8,128)(2,1)S(1)}, bf16[1032,128]{1,0:T(8,128)(2,1)S(1)}, u32[]{:S(2)}, u32[]{:S(2)}) collective-permute-start(bf16[1032,128]{1,0:T(8,128)(2,1)S(1)} %shard_map.146.refs_0_), channel_id=1, source_target_pairs={{0,16},{1,65},{2,18},{3,67},{4,20},{5,69},{6,22},{7,71},{8,24},{9,... | collective-permute-start | bytes 792584 | tf_op jit(solution)/shard_map/ppermute | solution.py:48
  20.5 6.9 %collective-permute-start.8 = (bf16[1032,128]{1,0:T(8,128)(2,1)S(1)}, bf16[1032,128]{1,0:T(8,128)(2,1)S(1)}, u32[]{:S(2)}, u32[]{:S(2)}) collective-permute-start(bf16[1032,128]{1,0:T(8,128)(2,1)S(1)} %shard_map.146.refs_0_), channel_id=1, source_target_pairs={{0,24},{1,97},{2,26},{3,99},{4,28},{5,101},{6,30},{7,103},{8,16},{... | collective-permute-start | bytes 792584 | tf_op jit(solution)/shard_map/ppermute | solution.py:48
  20.9 7.4 %collective-permute-start.9 = (bf16[1032,128]{1,0:T(8,128)(2,1)S(1)}, bf16[1032,128]{1,0:T(8,128)(2,1)S(1)}, u32[]{:S(2)}, u32[]{:S(2)}) collective-permute-start(bf16[1032,128]{1,0:T(8,128)(2,1)S(1)} %shard_map.146.refs_0_), channel_id=1, source_target_pairs={{0,8},{1,33},{2,10},{3,35},{4,12},{5,37},{6,14},{7,39},{8,0},{9,41... | collective-permute-start | bytes 792584 | tf_op jit(solution)/shard_map/ppermute | solution.py:48
  28.3 18.9 %copy-start.4 = (f32[192]{0:T(256)S(1)}, f32[192]{0:T(256)}, u32[]{:S(2)}) copy-start(f32[192]{0:T(256)} %param.22) | copy-start | bytes 2308
  28.7 4.0 %collective-permute-start.10 = (bf16[64,1024]{1,0:T(8,128)(2,1)S(1)}, bf16[64,1024]{1,0:T(8,128)(2,1)S(1)}, u32[]{:S(2)}, u32[]{:S(2)}) collective-permute-start(bf16[64,1024]{1,0:T(8,128)(2,1)S(1)} %shard_map.147.refs_0_), channel_id=1, source_target_pairs={{0,32},{1,9},{2,34},{3,11},{4,36},{5,13},{6,38},{7,15},{8,40},{9,1... | collective-permute-start | bytes 393224 | tf_op jit(solution)/shard_map/ppermute | solution.py:48
  30.1 6.4 %collective-permute-start.11 = (bf16[64,1024]{1,0:T(8,128)(2,1)S(1)}, bf16[64,1024]{1,0:T(8,128)(2,1)S(1)}, u32[]{:S(2)}, u32[]{:S(2)}) collective-permute-start(bf16[64,1024]{1,0:T(8,128)(2,1)S(1)} %shard_map.147.refs_0_), channel_id=1, source_target_pairs={{0,64},{1,17},{2,66},{3,19},{4,68},{5,21},{6,70},{7,23},{8,72},{9,... | collective-permute-start | bytes 393224 | tf_op jit(solution)/shard_map/ppermute | solution.py:48
  32.7 5.2 %collective-permute-start.12 = (bf16[64,1024]{1,0:T(8,128)(2,1)S(1)}, bf16[64,1024]{1,0:T(8,128)(2,1)S(1)}, u32[]{:S(2)}, u32[]{:S(2)}) collective-permute-start(bf16[64,1024]{1,0:T(8,128)(2,1)S(1)} %shard_map.147.refs_0_), channel_id=1, source_target_pairs={{0,96},{1,25},{2,98},{3,27},{4,100},{5,29},{6,102},{7,31},{8,104},... | collective-permute-start | bytes 393224 | tf_op jit(solution)/shard_map/ppermute | solution.py:48
  37.9 13.0 %copy-start.2 = (f32[192,1024]{1,0:T(8,128)S(1)}, f32[192,1024]{1,0:T(8,128)}, u32[]{:S(2)}) copy-start(f32[192,1024]{1,0:T(8,128)} %refs_0_.1) | copy-start | bytes 2359300
  37.9 13.1 %copy-start.3 = (f32[192,1024]{1,0:T(8,128)S(1)}, f32[192,1024]{1,0:T(8,128)}, u32[]{:S(2)}) copy-start(f32[192,1024]{1,0:T(8,128)} %refs_2_.1) | copy-start | bytes 2359300
  38.3 5.2 %collective-permute-start.13 = (bf16[192,128]{1,0:T(8,128)(2,1)S(1)}, bf16[192,128]{1,0:T(8,128)(2,1)S(1)}, u32[]{:S(2)}, u32[]{:S(2)}) collective-permute-start(bf16[192,128]{1,0:T(8,128)(2,1)S(1)} %get-tuple-element.37), channel_id=1, source_target_pairs={{0,1},{1,0},{2,3},{3,2},{4,5},{5,4},{6,7},{7,6},{8,9},{9,8},{10,11... | collective-permute-start | bytes 147464 | tf_op jit(solution)/shard_map/ppermute | solution.py:52
  43.5 4.5 %collective-permute-start.14 = (bf16[192,128]{1,0:T(8,128)(2,1)S(1)}, bf16[192,128]{1,0:T(8,128)(2,1)S(1)}, u32[]{:S(2)}, u32[]{:S(2)}) collective-permute-start(bf16[192,128]{1,0:T(8,128)(2,1)S(1)} %fusion.1), channel_id=1, source_target_pairs={{0,4},{1,5},{2,6},{3,7},{4,0},{5,1},{6,2},{7,3},{8,12},{9,13},{10,... | collective-permute-start | bytes 147464 | tf_op jit(solution)/shard_map/ppermute | solution.py:58
  46.4 3.1 %collective-permute-start.15 = (bf16[192,128]{1,0:T(8,128)(2,1)S(1)}, bf16[192,128]{1,0:T(8,128)(2,1)S(1)}, u32[]{:S(2)}, u32[]{:S(2)}) collective-permute-start(bf16[192,128]{1,0:T(8,128)(2,1)S(1)} %fusion.1), channel_id=1, source_target_pairs={{0,2},{1,3},{2,0},{3,1},{4,6},{5,7},{6,4},{7,5},{8,10},{9,11},{10,... | collective-permute-start | bytes 147464 | tf_op jit(solution)/shard_map/ppermute | solution.py:58
  46.7 4.2 %collective-permute-start.16 = (bf16[192,128]{1,0:T(8,128)(2,1)S(1)}, bf16[192,128]{1,0:T(8,128)(2,1)S(1)}, u32[]{:S(2)}, u32[]{:S(2)}) collective-permute-start(bf16[192,128]{1,0:T(8,128)(2,1)S(1)} %fusion.1), channel_id=1, source_target_pairs={{0,6},{1,7},{2,4},{3,5},{4,2},{5,3},{6,0},{7,1},{8,14},{9,15},{10,... | collective-permute-start | bytes 147464 | tf_op jit(solution)/shard_map/ppermute | solution.py:58
  51.5 7.1 %collective-permute-start.17 = (bf16[1032,128]{1,0:T(8,128)(2,1)S(1)}, bf16[1032,128]{1,0:T(8,128)(2,1)S(1)}, u32[]{:S(2)}, u32[]{:S(2)}) collective-permute-start(bf16[1032,128]{1,0:T(8,128)(2,1)S(1)} %get-tuple-element.42), channel_id=1, source_target_pairs={{0,64},{1,17},{2,66},{3,19},{4,68},{5,21},{6,70},{7,23},{8,72},{9,... | collective-permute-start | bytes 792584 | tf_op jit(solution)/shard_map/ppermute | solution.py:48
  53.3 8.1 %collective-permute-start.18 = (bf16[1032,128]{1,0:T(8,128)(2,1)S(1)}, bf16[1032,128]{1,0:T(8,128)(2,1)S(1)}, u32[]{:S(2)}, u32[]{:S(2)}) collective-permute-start(bf16[1032,128]{1,0:T(8,128)(2,1)S(1)} %get-tuple-element.43), channel_id=1, source_target_pairs={{0,96},{1,25},{2,98},{3,27},{4,100},{5,29},{6,102},{7,31},{8,104},... | collective-permute-start | bytes 792584 | tf_op jit(solution)/shard_map/ppermute | solution.py:48
  55.0 6.4 %collective-permute-start.19 = (bf16[1032,128]{1,0:T(8,128)(2,1)S(1)}, bf16[1032,128]{1,0:T(8,128)(2,1)S(1)}, u32[]{:S(2)}, u32[]{:S(2)}) collective-permute-start(bf16[1032,128]{1,0:T(8,128)(2,1)S(1)} %get-tuple-element.44), channel_id=1, source_target_pairs={{0,32},{1,9},{2,34},{3,11},{4,36},{5,13},{6,38},{7,15},{8,40},{9,1... | collective-permute-start | bytes 792584 | tf_op jit(solution)/shard_map/ppermute | solution.py:48
  61.7 18.9 %copy-start.1 = (f32[1024,192]{0,1:T(8,128)S(1)}, f32[1024,192]{0,1:T(8,128)}, u32[]{:S(2)}) copy-start(f32[1024,192]{0,1:T(8,128)} %param.26) | copy-start | bytes 2359300
  61.7 6.9 %collective-permute-start.20 = (bf16[1032,128]{1,0:T(8,128)(2,1)S(1)}, bf16[1032,128]{1,0:T(8,128)(2,1)S(1)}, u32[]{:S(2)}, u32[]{:S(2)}) collective-permute-start(bf16[1032,128]{1,0:T(8,128)(2,1)S(1)} %shard_map.150.refs_0_), channel_id=1, source_target_pairs={{0,16},{1,65},{2,18},{3,67},{4,20},{5,69},{6,22},{7,71},{8,24},{9,... | collective-permute-start | bytes 792584 | tf_op jit(solution)/shard_map/ppermute | solution.py:48
  61.9 9.6 %collective-permute-start.21 = (bf16[1032,128]{1,0:T(8,128)(2,1)S(1)}, bf16[1032,128]{1,0:T(8,128)(2,1)S(1)}, u32[]{:S(2)}, u32[]{:S(2)}) collective-permute-start(bf16[1032,128]{1,0:T(8,128)(2,1)S(1)} %shard_map.150.refs_0_), channel_id=1, source_target_pairs={{0,24},{1,97},{2,26},{3,99},{4,28},{5,101},{6,30},{7,103},{8,16},{... | collective-permute-start | bytes 792584 | tf_op jit(solution)/shard_map/ppermute | solution.py:48
  63.3 8.2 %collective-permute-start.22 = (bf16[1032,128]{1,0:T(8,128)(2,1)S(1)}, bf16[1032,128]{1,0:T(8,128)(2,1)S(1)}, u32[]{:S(2)}, u32[]{:S(2)}) collective-permute-start(bf16[1032,128]{1,0:T(8,128)(2,1)S(1)} %shard_map.150.refs_0_), channel_id=1, source_target_pairs={{0,8},{1,33},{2,10},{3,35},{4,12},{5,37},{6,14},{7,39},{8,0},{9,41... | collective-permute-start | bytes 792584 | tf_op jit(solution)/shard_map/ppermute | solution.py:48
  71.9 12.6 %copy-start.5 = (f32[192]{0:T(256)S(1)}, f32[192]{0:T(256)}, u32[]{:S(2)}) copy-start(f32[192]{0:T(256)} %param.29) | copy-start | bytes 2308
  71.9 4.3 %collective-permute-start.23 = (bf16[32,2048]{1,0:T(8,128)(2,1)S(1)}, bf16[32,2048]{1,0:T(8,128)(2,1)S(1)}, u32[]{:S(2)}, u32[]{:S(2)}) collective-permute-start(bf16[32,2048]{1,0:T(8,128)(2,1)S(1)} %shard_map.151.refs_0_), channel_id=1, source_target_pairs={{0,32},{1,9},{2,34},{3,11},{4,36},{5,13},{6,38},{7,15},{8,40},{9,1... | collective-permute-start | bytes 393224 | tf_op jit(solution)/shard_map/ppermute | solution.py:48
  72.9 6.4 %collective-permute-start.24 = (bf16[32,2048]{1,0:T(8,128)(2,1)S(1)}, bf16[32,2048]{1,0:T(8,128)(2,1)S(1)}, u32[]{:S(2)}, u32[]{:S(2)}) collective-permute-start(bf16[32,2048]{1,0:T(8,128)(2,1)S(1)} %shard_map.151.refs_0_), channel_id=1, source_target_pairs={{0,64},{1,17},{2,66},{3,19},{4,68},{5,21},{6,70},{7,23},{8,72},{9,... | collective-permute-start | bytes 393224 | tf_op jit(solution)/shard_map/ppermute | solution.py:48
  75.5 5.2 %collective-permute-start.25 = (bf16[32,2048]{1,0:T(8,128)(2,1)S(1)}, bf16[32,2048]{1,0:T(8,128)(2,1)S(1)}, u32[]{:S(2)}, u32[]{:S(2)}) collective-permute-start(bf16[32,2048]{1,0:T(8,128)(2,1)S(1)} %shard_map.151.refs_0_), channel_id=1, source_target_pairs={{0,96},{1,25},{2,98},{3,27},{4,100},{5,29},{6,102},{7,31},{8,104},... | collective-permute-start | bytes 393224 | tf_op jit(solution)/shard_map/ppermute | solution.py:48
  81.1 4.5 %collective-permute-start.26 = (bf16[192,128]{1,0:T(8,128)(2,1)S(1)}, bf16[192,128]{1,0:T(8,128)(2,1)S(1)}, u32[]{:S(2)}, u32[]{:S(2)}) collective-permute-start(bf16[192,128]{1,0:T(8,128)(2,1)S(1)} %shard_map.152), channel_id=1, source_target_pairs={{0,4},{1,5},{2,6},{3,7},{4,0},{5,1},{6,2},{7,3},{8,12},{9,13},{10,... | collective-permute-start | bytes 147464 | tf_op jit(solution)/shard_map/ppermute | solution.py:58
  82.6 3.1 %collective-permute-start.27 = (bf16[192,128]{1,0:T(8,128)(2,1)S(1)}, bf16[192,128]{1,0:T(8,128)(2,1)S(1)}, u32[]{:S(2)}, u32[]{:S(2)}) collective-permute-start(bf16[192,128]{1,0:T(8,128)(2,1)S(1)} %shard_map.152), channel_id=1, source_target_pairs={{0,2},{1,3},{2,0},{3,1},{4,6},{5,7},{6,4},{7,5},{8,10},{9,11},{10,... | collective-permute-start | bytes 147464 | tf_op jit(solution)/shard_map/ppermute | solution.py:58
  83.1 4.2 %collective-permute-start.28 = (bf16[192,128]{1,0:T(8,128)(2,1)S(1)}, bf16[192,128]{1,0:T(8,128)(2,1)S(1)}, u32[]{:S(2)}, u32[]{:S(2)}) collective-permute-start(bf16[192,128]{1,0:T(8,128)(2,1)S(1)} %shard_map.152), channel_id=1, source_target_pairs={{0,6},{1,7},{2,4},{3,5},{4,2},{5,3},{6,0},{7,1},{8,14},{9,15},{10,... | collective-permute-start | bytes 147464 | tf_op jit(solution)/shard_map/ppermute | solution.py:58
  87.4 5.2 %collective-permute-start.29 = (bf16[192,128]{1,0:T(8,128)(2,1)S(1)}, bf16[192,128]{1,0:T(8,128)(2,1)S(1)}, u32[]{:S(2)}, u32[]{:S(2)}) collective-permute-start(bf16[192,128]{1,0:T(8,128)(2,1)S(1)} %add_convert_fusion), channel_id=1, source_target_pairs={{0,1},{1,0},{2,3},{3,2},{4,5},{5,4},{6,7},{7,6},{8,9},{9,8},{10,11... | collective-permute-start | bytes 147464 | tf_op jit(solution)/shard_map/ppermute | solution.py:52

commit v2 on v1

--- a/solution.py
+++ b/solution.py
@@ -10,7 +10,7 @@
 
 D = 3072
 SIDE = 4
-WIDE = 1024
+WIDE = 512
 PIECE = 96
 ORDER = (2, 3, 1)
 X_ORDER = (2, 3, 1)
@@ -116,7 +116,7 @@
         pltpu.make_async_copy(ref, target, small_sems.at[k])
         for k, (ref, target) in enumerate(zip((stream_ref, gain_ref, *small_refs), targets, strict=True))
     ]
-    for copy in small[:2]:
+    for copy in small:
         copy.start()
     copies = [
         pltpu.make_async_copy(ref.at[pl.ds(at, PIECE)], held.at[n, pl.ds(at, PIECE)], sems.at[n, at // PIECE])
@@ -124,8 +124,6 @@
         for at in range(0, ref.shape[0], PIECE)
     ]
     for copy in copies:
-        copy.start()
-    for copy in small[2:]:
         copy.start()
 
     def piece(n, at):

time: 93.3 us -> 93.3 us (level)
  no operation moved by 1% of the time
where the time goes in v2:
time: 93.3 us; the launch traced here: 93.1 us
  waiting for transfers between devices  44 us (47%)
  starting transfers between devices  43.4 us (47%)
  Pallas kernels  4.65 us (5%)
    ppermute x18, waiting for transfers between devices, swapped(): return lax.ppermute(x, ('ra', 'cb'), pairs_of(k, along_f))  35 us
    ppermute x18, starting transfers between devices, swapped(): return lax.ppermute(x, ('ra', 'cb'), pairs_of(k, along_f))  25 us
    ppermute x6, starting transfers between devices, other_core(): lax.ppermute(x, 'cb', [(i, i ^ 1) for i in range(lax.axis_size('cb'))])  11.4 us
    ppermute x6, starting transfers between devices, sum_over_x(): lax.ppermute(sent, 'cb', [(i, i ^ 2 * k) for i in range(n)]).astype(F32)  7.02 us
    ppermute x6, waiting for transfers between devices, sum_over_x(): lax.ppermute(sent, 'cb', [(i, i ^ 2 * k) for i in range(n)]).astype(F32)  6.42 us
    ppermute x6, waiting for transfers between devices, other_core(): lax.ppermute(x, 'cb', [(i, i ^ 1) for i in range(lax.axis_size('cb'))])  2.6 us
    pallas_call x2, Pallas kernels, products(): pl.pallas_call(fetching_kernel if small else products_kernel, out_shape=o...  2.45 us
    pallas_call x6, Pallas kernels, call(): pl.pallas_call(kernel, out_shape=[jax.ShapeDtypeStruct(shape, BF16) for s...  2.2 us
  transfers between devices with their start and end apart: 30, of which 22 were waited for; matrix products, arithmetic and copies ran while one was open for 0% of the time, Pallas kernels for 2%

profile of v2, /device:TPU:1, one launch (start us, length us, event | category | flops | bytes accessed | tf_op | source)
XLA Modules:
  0.0 93.1 jit_solution(5694306556469253111)
XLA Ops:
  0.0 1.4 %collective-permute-start.5 = (f32[192,1024]{1,0:T(8,128)}, f32[192,1024]{1,0:T(8,128)S(1)}, u32[]{:S(2)}, u32[]{:S(2)}) collective-permute-start(f32[192,1024]{1,0:T(8,128)} %bitcast.12), channel_id=1, source_target_pairs={{0,1},{1,0},{2,3},{3,2},{4,5},{5,4},{6,7},{7,6},{8,9},{9,8},{10,11... | collective-permute-start | bytes 2359304 | tf_op jit(solution)/shard_map/ppermute | solution.py:52
  1.4 0.0 collective-permute-start.3
  1.4 0.5 collective-permute-start.4
  1.9 1.9 %shard_map.145 = (bf16[1032,128]{1,0:T(8,128)(2,1)S(1)}, bf16[1032,128]{1,0:T(8,128)(2,1)S(1)}, bf16[1032,128]{1,0:T(8,128)(2,1)S(1)}, bf16[1032,128]{1,0:T(8,12...) custom-call(bf16[192,256]{1,0:T(8,128)(2,1)} %bitcast.14, ...), custom_call_target="tpu_custom_call" | custom-call | flops 201326592 | bytes 1572864 | tf_op jit(solution)/shard_map/pallas_call | solution.py:175
  3.8 3.1 %collective-permute-start = (bf16[1032,128]{1,0:T(8,128)(2,1)S(1)}, bf16[1032,128]{1,0:T(8,128)(2,1)S(1)}, u32[]{:S(2)}, u32[]{:S(2)}) collective-permute-start(bf16[1032,128]{1,0:T(8,128)(2,1)S(1)} %get-tuple-element.28), channel_id=1, source_target_pairs={{0,64},{1,17},{2,66},{3,19},{4,68},{5,21},{6,70},{7,23},{8,72},{9,... | collective-permute-start | bytes 792584 | tf_op jit(solution)/shard_map/ppermute | solution.py:48
  6.9 1.0 %collective-permute-start.6 = (f32[2,1,1024]{2,1,0:T(1,128)S(1)}, f32[2,1,1024]{2,1,0:T(1,128)S(1)}, u32[]{:S(2)}, u32[]{:S(2)}) collective-permute-start(f32[2,1,1024]{2,1,0:T(1,128)S(1)} %get-tuple-element.31.refs_4_), channel_id=1, source_target_pairs={{0,1},{1,0},{2,3},{3,2},{4,5},{5,4},{6,7},{7,6},{8,9},{9,8},{10,11... | collective-permute-start | bytes 24584 | tf_op jit(solution)/shard_map/ppermute | solution.py:52
  7.9 0.8 collective-permute-done.6.refs_5_
  8.7 2.7 %collective-permute-start.1 = (bf16[1032,128]{1,0:T(8,128)(2,1)S(1)}, bf16[1032,128]{1,0:T(8,128)(2,1)S(1)}, u32[]{:S(2)}, u32[]{:S(2)}) collective-permute-start(bf16[1032,128]{1,0:T(8,128)(2,1)S(1)} %get-tuple-element.29), channel_id=1, source_target_pairs={{0,96},{1,25},{2,98},{3,27},{4,100},{5,29},{6,102},{7,31},{8,104},... | collective-permute-start | bytes 792584 | tf_op jit(solution)/shard_map/ppermute | solution.py:48
  11.5 0.9 collective-permute-start.2
  12.4 3.2 %collective-permute-done.1.refs_2_ = bf16[1032,128]{1,0:T(8,128)(2,1)S(1)} collective-permute-done((bf16[1032,128]{1,0:T(8,128)(2,1)S(1)}, bf16[1032,128]{1,0:T(8,128)(2,1)S(1)}, u32[]{:S(2)}, u32[]{:S(2)}) %collective-permute-start.1) | collective-permute-done | bytes 264224 | tf_op jit(solution)/shard_map/ppermute | solution.py:48
  15.5 1.5 %collective-permute-done.2.refs_3_ = bf16[1032,128]{1,0:T(8,128)(2,1)S(1)} collective-permute-done((bf16[1032,128]{1,0:T(8,128)(2,1)S(1)}, bf16[1032,128]{1,0:T(8,128)(2,1)S(1)}, u32[]{:S(2)}, u32[]{:S(2)}) %collective-permute-start.2) | collective-permute-done | bytes 264224 | tf_op jit(solution)/shard_map/ppermute | solution.py:48
  17.0 0.3 shard_map.146.refs_0_
  17.3 0.0 copy-start
  17.3 3.1 %collective-permute-start.7 = (bf16[1032,128]{1,0:T(8,128)(2,1)S(1)}, bf16[1032,128]{1,0:T(8,128)(2,1)S(1)}, u32[]{:S(2)}, u32[]{:S(2)}) collective-permute-start(bf16[1032,128]{1,0:T(8,128)(2,1)S(1)} %shard_map.146.refs_0_), channel_id=1, source_target_pairs={{0,16},{1,65},{2,18},{3,67},{4,20},{5,69},{6,22},{7,71},{8,24},{9,... | collective-permute-start | bytes 792584 | tf_op jit(solution)/shard_map/ppermute | solution.py:48
  20.4 0.4 collective-permute-start.8
  20.9 0.5 collective-permute-start.9
  21.3 3.2 %collective-permute-done.7.refs_1_ = bf16[1032,128]{1,0:T(8,128)(2,1)S(1)} collective-permute-done((bf16[1032,128]{1,0:T(8,128)(2,1)S(1)}, bf16[1032,128]{1,0:T(8,128)(2,1)S(1)}, u32[]{:S(2)}, u32[]{:S(2)}) %collective-permute-start.7) | collective-permute-done | bytes 264224 | tf_op jit(solution)/shard_map/ppermute | solution.py:48
  24.5 2.8 %collective-permute-done.8.refs_2_ = bf16[1032,128]{1,0:T(8,128)(2,1)S(1)} collective-permute-done((bf16[1032,128]{1,0:T(8,128)(2,1)S(1)}, bf16[1032,128]{1,0:T(8,128)(2,1)S(1)}, u32[]{:S(2)}, u32[]{:S(2)}) %collective-permute-start.8) | collective-permute-done | bytes 264224 | tf_op jit(solution)/shard_map/ppermute | solution.py:48
  27.3 0.9 %collective-permute-done.9.refs_3_ = bf16[1032,128]{1,0:T(8,128)(2,1)S(1)} collective-permute-done((bf16[1032,128]{1,0:T(8,128)(2,1)S(1)}, bf16[1032,128]{1,0:T(8,128)(2,1)S(1)}, u32[]{:S(2)}, u32[]{:S(2)}) %collective-permute-start.9) | collective-permute-done | bytes 264224 | tf_op jit(solution)/shard_map/ppermute | solution.py:48
  28.3 0.4 shard_map.147.refs_0_
  28.7 1.4 %collective-permute-start.10 = (bf16[64,1024]{1,0:T(8,128)(2,1)S(1)}, bf16[64,1024]{1,0:T(8,128)(2,1)S(1)}, u32[]{:S(2)}, u32[]{:S(2)}) collective-permute-start(bf16[64,1024]{1,0:T(8,128)(2,1)S(1)} %shard_map.147.refs_0_), channel_id=1, source_target_pairs={{0,32},{1,9},{2,34},{3,11},{4,36},{5,13},{6,38},{7,15},{8,40},{9,1... | collective-permute-start | bytes 393224 | tf_op jit(solution)/shard_map/ppermute | solution.py:48
  30.1 2.6 %collective-permute-start.11 = (bf16[64,1024]{1,0:T(8,128)(2,1)S(1)}, bf16[64,1024]{1,0:T(8,128)(2,1)S(1)}, u32[]{:S(2)}, u32[]{:S(2)}) collective-permute-start(bf16[64,1024]{1,0:T(8,128)(2,1)S(1)} %shard_map.147.refs_0_), channel_id=1, source_target_pairs={{0,64},{1,17},{2,66},{3,19},{4,68},{5,21},{6,70},{7,23},{8,72},{9,... | collective-permute-start | bytes 393224 | tf_op jit(solution)/shard_map/ppermute | solution.py:48
  32.7 3.8 %collective-permute-done.11.refs_2_ = bf16[64,1024]{1,0:T(8,128)(2,1)S(1)} collective-permute-done((bf16[64,1024]{1,0:T(8,128)(2,1)S(1)}, bf16[64,1024]{1,0:T(8,128)(2,1)S(1)}, u32[]{:S(2)}, u32[]{:S(2)}) %collective-permute-start.11) | collective-permute-done | bytes 131104 | tf_op jit(solution)/shard_map/ppermute | solution.py:48
  36.4 1.4 %collective-permute-done.12.refs_3_ = bf16[64,1024]{1,0:T(8,128)(2,1)S(1)} collective-permute-done((bf16[64,1024]{1,0:T(8,128)(2,1)S(1)}, bf16[64,1024]{1,0:T(8,128)(2,1)S(1)}, u32[]{:S(2)}, u32[]{:S(2)}) %collective-permute-start.12) | collective-permute-done | bytes 131104 | tf_op jit(solution)/shard_map/ppermute | solution.py:48
  37.8 0.4 shard_map.148
  38.3 4.3 %collective-permute-start.13 = (bf16[192,128]{1,0:T(8,128)(2,1)S(1)}, bf16[192,128]{1,0:T(8,128)(2,1)S(1)}, u32[]{:S(2)}, u32[]{:S(2)}) collective-permute-start(bf16[192,128]{1,0:T(8,128)(2,1)S(1)} %get-tuple-element.37), channel_id=1, source_target_pairs={{0,1},{1,0},{2,3},{3,2},{4,5},{5,4},{6,7},{7,6},{8,9},{9,8},{10,11... | collective-permute-start | bytes 147464 | tf_op jit(solution)/shard_map/ppermute | solution.py:52
  42.6 0.9 collective-permute-done.13
  43.5 2.8 %collective-permute-start.14 = (bf16[192,128]{1,0:T(8,128)(2,1)S(1)}, bf16[192,128]{1,0:T(8,128)(2,1)S(1)}, u32[]{:S(2)}, u32[]{:S(2)}) collective-permute-start(bf16[192,128]{1,0:T(8,128)(2,1)S(1)} %fusion.1), channel_id=1, source_target_pairs={{0,4},{1,5},{2,6},{3,7},{4,0},{5,1},{6,2},{7,3},{8,12},{9,13},{10,... | collective-permute-start | bytes 147464 | tf_op jit(solution)/shard_map/ppermute | solution.py:58
  46.3 0.3 collective-permute-start.15
  46.6 0.5 collective-permute-start.16
  47.2 0.8 collective-permute-done.14
  48.0 1.4 %collective-permute-done.15 = bf16[192,128]{1,0:T(8,128)(2,1)S(1)} collective-permute-done((bf16[192,128]{1,0:T(8,128)(2,1)S(1)}, bf16[192,128]{1,0:T(8,128)(2,1)S(1)}, u32[]{:S(2)}, u32[]{:S(2)}) %collective-permute-start.15) | collective-permute-done | bytes 49184 | tf_op jit(solution)/shard_map/ppermute | solution.py:58
  49.4 1.3 %collective-permute-done.16 = bf16[192,128]{1,0:T(8,128)(2,1)S(1)} collective-permute-done((bf16[192,128]{1,0:T(8,128)(2,1)S(1)}, bf16[192,128]{1,0:T(8,128)(2,1)S(1)}, u32[]{:S(2)}, u32[]{:S(2)}) %collective-permute-start.16) | collective-permute-done | bytes 49184 | tf_op jit(solution)/shard_map/ppermute | solution.py:58
  50.8 0.1 add_convert_fusion.1.stream_ref
  50.9 0.5 shard_map.149
  51.4 1.8 %collective-permute-start.17 = (bf16[1032,128]{1,0:T(8,128)(2,1)S(1)}, bf16[1032,128]{1,0:T(8,128)(2,1)S(1)}, u32[]{:S(2)}, u32[]{:S(2)}) collective-permute-start(bf16[1032,128]{1,0:T(8,128)(2,1)S(1)} %get-tuple-element.42), channel_id=1, source_target_pairs={{0,64},{1,17},{2,66},{3,19},{4,68},{5,21},{6,70},{7,23},{8,72},{9,... | collective-permute-start | bytes 792584 | tf_op jit(solution)/shard_map/ppermute | solution.py:48
  53.3 1.7 %collective-permute-start.18 = (bf16[1032,128]{1,0:T(8,128)(2,1)S(1)}, bf16[1032,128]{1,0:T(8,128)(2,1)S(1)}, u32[]{:S(2)}, u32[]{:S(2)}) collective-permute-start(bf16[1032,128]{1,0:T(8,128)(2,1)S(1)} %get-tuple-element.43), channel_id=1, source_target_pairs={{0,96},{1,25},{2,98},{3,27},{4,100},{5,29},{6,102},{7,31},{8,104},... | collective-permute-start | bytes 792584 | tf_op jit(solution)/shard_map/ppermute | solution.py:48
  55.0 3.6 %collective-permute-done.17.refs_1_ = bf16[1032,128]{1,0:T(8,128)(2,1)S(1)} collective-permute-done((bf16[1032,128]{1,0:T(8,128)(2,1)S(1)}, bf16[1032,128]{1,0:T(8,128)(2,1)S(1)}, u32[]{:S(2)}, u32[]{:S(2)}) %collective-permute-start.17) | collective-permute-done | bytes 264224 | tf_op jit(solution)/shard_map/ppermute | solution.py:48
  58.6 2.8 %collective-permute-done.18.refs_2_ = bf16[1032,128]{1,0:T(8,128)(2,1)S(1)} collective-permute-done((bf16[1032,128]{1,0:T(8,128)(2,1)S(1)}, bf16[1032,128]{1,0:T(8,128)(2,1)S(1)}, u32[]{:S(2)}, u32[]{:S(2)}) %collective-permute-start.18) | collective-permute-done | bytes 264224 | tf_op jit(solution)/shard_map/ppermute | solution.py:48
  61.4 0.3 shard_map.150.refs_0_
  61.7 0.0 copy-start.1
  61.7 0.1 collective-permute-start.20
  61.8 1.5 %collective-permute-start.21 = (bf16[1032,128]{1,0:T(8,128)(2,1)S(1)}, bf16[1032,128]{1,0:T(8,128)(2,1)S(1)}, u32[]{:S(2)}, u32[]{:S(2)}) collective-permute-start(bf16[1032,128]{1,0:T(8,128)(2,1)S(1)} %shard_map.150.refs_0_), channel_id=1, source_target_pairs={{0,24},{1,97},{2,26},{3,99},{4,28},{5,101},{6,30},{7,103},{8,16},{... | collective-permute-start | bytes 792584 | tf_op jit(solution)/shard_map/ppermute | solution.py:48
  63.3 1.2 %collective-permute-start.22 = (bf16[1032,128]{1,0:T(8,128)(2,1)S(1)}, bf16[1032,128]{1,0:T(8,128)(2,1)S(1)}, u32[]{:S(2)}, u32[]{:S(2)}) collective-permute-start(bf16[1032,128]{1,0:T(8,128)(2,1)S(1)} %shard_map.150.refs_0_), channel_id=1, source_target_pairs={{0,8},{1,33},{2,10},{3,35},{4,12},{5,37},{6,14},{7,39},{8,0},{9,41... | collective-permute-start | bytes 792584 | tf_op jit(solution)/shard_map/ppermute | solution.py:48
  64.4 4.2 %collective-permute-done.20.refs_1_ = bf16[1032,128]{1,0:T(8,128)(2,1)S(1)} collective-permute-done((bf16[1032,128]{1,0:T(8,128)(2,1)S(1)}, bf16[1032,128]{1,0:T(8,128)(2,1)S(1)}, u32[]{:S(2)}, u32[]{:S(2)}) %collective-permute-start.20) | collective-permute-done | bytes 264224 | tf_op jit(solution)/shard_map/ppermute | solution.py:48
  68.6 2.8 %collective-permute-done.21.refs_2_ = bf16[1032,128]{1,0:T(8,128)(2,1)S(1)} collective-permute-done((bf16[1032,128]{1,0:T(8,128)(2,1)S(1)}, bf16[1032,128]{1,0:T(8,128)(2,1)S(1)}, u32[]{:S(2)}, u32[]{:S(2)}) %collective-permute-start.21) | collective-permute-done | bytes 264224 | tf_op jit(solution)/shard_map/ppermute | solution.py:48
  71.4 0.4 shard_map.151.refs_0_
  71.8 0.0 copy-start.5
  71.8 1.0 %collective-permute-start.23 = (bf16[32,2048]{1,0:T(8,128)(2,1)S(1)}, bf16[32,2048]{1,0:T(8,128)(2,1)S(1)}, u32[]{:S(2)}, u32[]{:S(2)}) collective-permute-start(bf16[32,2048]{1,0:T(8,128)(2,1)S(1)} %shard_map.151.refs_0_), channel_id=1, source_target_pairs={{0,32},{1,9},{2,34},{3,11},{4,36},{5,13},{6,38},{7,15},{8,40},{9,1... | collective-permute-start | bytes 393224 | tf_op jit(solution)/shard_map/ppermute | solution.py:48
  72.8 2.6 %collective-permute-start.24 = (bf16[32,2048]{1,0:T(8,128)(2,1)S(1)}, bf16[32,2048]{1,0:T(8,128)(2,1)S(1)}, u32[]{:S(2)}, u32[]{:S(2)}) collective-permute-start(bf16[32,2048]{1,0:T(8,128)(2,1)S(1)} %shard_map.151.refs_0_), channel_id=1, source_target_pairs={{0,64},{1,17},{2,66},{3,19},{4,68},{5,21},{6,70},{7,23},{8,72},{9,... | collective-permute-start | bytes 393224 | tf_op jit(solution)/shard_map/ppermute | solution.py:48
  75.5 0.3 collective-permute-start.25
  75.8 0.3 collective-permute-done.23.refs_1_
  76.1 3.1 %collective-permute-done.24.refs_2_ = bf16[32,2048]{1,0:T(8,128)(2,1)S(1)} collective-permute-done((bf16[32,2048]{1,0:T(8,128)(2,1)S(1)}, bf16[32,2048]{1,0:T(8,128)(2,1)S(1)}, u32[]{:S(2)}, u32[]{:S(2)}) %collective-permute-start.24) | collective-permute-done | bytes 131104 | tf_op jit(solution)/shard_map/ppermute | solution.py:48
  79.2 1.4 %collective-permute-done.25.refs_3_ = bf16[32,2048]{1,0:T(8,128)(2,1)S(1)} collective-permute-done((bf16[32,2048]{1,0:T(8,128)(2,1)S(1)}, bf16[32,2048]{1,0:T(8,128)(2,1)S(1)}, u32[]{:S(2)}, u32[]{:S(2)}) %collective-permute-start.25) | collective-permute-done | bytes 131104 | tf_op jit(solution)/shard_map/ppermute | solution.py:48
  80.6 0.4 shard_map.152
  81.1 1.4 %collective-permute-start.26 = (bf16[192,128]{1,0:T(8,128)(2,1)S(1)}, bf16[192,128]{1,0:T(8,128)(2,1)S(1)}, u32[]{:S(2)}, u32[]{:S(2)}) collective-permute-start(bf16[192,128]{1,0:T(8,128)(2,1)S(1)} %shard_map.152), channel_id=1, source_target_pairs={{0,4},{1,5},{2,6},{3,7},{4,0},{5,1},{6,2},{7,3},{8,12},{9,13},{10,... | collective-permute-start | bytes 147464 | tf_op jit(solution)/shard_map/ppermute | solution.py:58
  82.5 0.6 collective-permute-start.27
  83.1 1.3 %collective-permute-start.28 = (bf16[192,128]{1,0:T(8,128)(2,1)S(1)}, bf16[192,128]{1,0:T(8,128)(2,1)S(1)}, u32[]{:S(2)}, u32[]{:S(2)}) collective-permute-start(bf16[192,128]{1,0:T(8,128)(2,1)S(1)} %shard_map.152), channel_id=1, source_target_pairs={{0,6},{1,7},{2,4},{3,5},{4,2},{5,3},{6,0},{7,1},{8,14},{9,15},{10,... | collective-permute-start | bytes 147464 | tf_op jit(solution)/shard_map/ppermute | solution.py:58
  84.4 1.2 %collective-permute-done.26 = bf16[192,128]{1,0:T(8,128)(2,1)S(1)} collective-permute-done((bf16[192,128]{1,0:T(8,128)(2,1)S(1)}, bf16[192,128]{1,0:T(8,128)(2,1)S(1)}, u32[]{:S(2)}, u32[]{:S(2)}) %collective-permute-start.26) | collective-permute-done | bytes 49184 | tf_op jit(solution)/shard_map/ppermute | solution.py:58
  85.6 1.6 %collective-permute-done.28 = bf16[192,128]{1,0:T(8,128)(2,1)S(1)} collective-permute-done((bf16[192,128]{1,0:T(8,128)(2,1)S(1)}, bf16[192,128]{1,0:T(8,128)(2,1)S(1)}, u32[]{:S(2)}, u32[]{:S(2)}) %collective-permute-start.28) | collective-permute-done | bytes 49184 | tf_op jit(solution)/shard_map/ppermute | solution.py:58
  87.2 0.1 add_convert_fusion
  87.3 4.3 %collective-permute-start.29 = (bf16[192,128]{1,0:T(8,128)(2,1)S(1)}, bf16[192,128]{1,0:T(8,128)(2,1)S(1)}, u32[]{:S(2)}, u32[]{:S(2)}) collective-permute-start(bf16[192,128]{1,0:T(8,128)(2,1)S(1)} %add_convert_fusion), channel_id=1, source_target_pairs={{0,1},{1,0},{2,3},{3,2},{4,5},{5,4},{6,7},{7,6},{8,9},{9,8},{10,11... | collective-permute-start | bytes 147464 | tf_op jit(solution)/shard_map/ppermute | solution.py:52
  91.6 0.9 collective-permute-done.29
  92.5 0.7 fusion
  (22 shorter events, 0.1 us)
Async XLA Ops:
  0.0 17.0 %collective-permute-start.5 = (f32[192,1024]{1,0:T(8,128)}, f32[192,1024]{1,0:T(8,128)S(1)}, u32[]{:S(2)}, u32[]{:S(2)}) collective-permute-start(f32[192,1024]{1,0:T(8,128)} %bitcast.12), channel_id=1, source_target_pairs={{0,1},{1,0},{2,3},{3,2},{4,5},{5,4},{6,7},{7,6},{8,9},{9,8},{10,11... | collective-permute-start | bytes 2359304 | tf_op jit(solution)/shard_map/ppermute | solution.py:52
  1.4 15.6 %collective-permute-start.3 = (f32[192,1024]{1,0:T(8,128)}, f32[192,1024]{1,0:T(8,128)S(1)}, u32[]{:S(2)}, u32[]{:S(2)}) collective-permute-start(f32[192,1024]{1,0:T(8,128)} %refs_0_.1), channel_id=1, source_target_pairs={{0,1},{1,0},{2,3},{3,2},{4,5},{5,4},{6,7},{7,6},{8,9},{9,8},{10,11... | collective-permute-start | bytes 2359304 | tf_op jit(solution)/shard_map/ppermute | solution.py:52
  1.4 15.6 %collective-permute-start.4 = (f32[192,1024]{1,0:T(8,128)}, f32[192,1024]{1,0:T(8,128)S(1)}, u32[]{:S(2)}, u32[]{:S(2)}) collective-permute-start(f32[192,1024]{1,0:T(8,128)} %refs_2_.1), channel_id=1, source_target_pairs={{0,1},{1,0},{2,3},{3,2},{4,5},{5,4},{6,7},{7,6},{8,9},{9,8},{10,11... | collective-permute-start | bytes 2359304 | tf_op jit(solution)/shard_map/ppermute | solution.py:52
  3.8 7.6 %collective-permute-start = (bf16[1032,128]{1,0:T(8,128)(2,1)S(1)}, bf16[1032,128]{1,0:T(8,128)(2,1)S(1)}, u32[]{:S(2)}, u32[]{:S(2)}) collective-permute-start(bf16[1032,128]{1,0:T(8,128)(2,1)S(1)} %get-tuple-element.28), channel_id=1, source_target_pairs={{0,64},{1,17},{2,66},{3,19},{4,68},{5,21},{6,70},{7,23},{8,72},{9,... | collective-permute-start | bytes 792584 | tf_op jit(solution)/shard_map/ppermute | solution.py:48
  6.9 1.8 %collective-permute-start.6 = (f32[2,1,1024]{2,1,0:T(1,128)S(1)}, f32[2,1,1024]{2,1,0:T(1,128)S(1)}, u32[]{:S(2)}, u32[]{:S(2)}) collective-permute-start(f32[2,1,1024]{2,1,0:T(1,128)S(1)} %get-tuple-element.31.refs_4_), channel_id=1, source_target_pairs={{0,1},{1,0},{2,3},{3,2},{4,5},{5,4},{6,7},{7,6},{8,9},{9,8},{10,11... | collective-permute-start | bytes 24584 | tf_op jit(solution)/shard_map/ppermute | solution.py:52
  8.7 6.8 %collective-permute-start.1 = (bf16[1032,128]{1,0:T(8,128)(2,1)S(1)}, bf16[1032,128]{1,0:T(8,128)(2,1)S(1)}, u32[]{:S(2)}, u32[]{:S(2)}) collective-permute-start(bf16[1032,128]{1,0:T(8,128)(2,1)S(1)} %get-tuple-element.29), channel_id=1, source_target_pairs={{0,96},{1,25},{2,98},{3,27},{4,100},{5,29},{6,102},{7,31},{8,104},... | collective-permute-start | bytes 792584 | tf_op jit(solution)/shard_map/ppermute | solution.py:48
  11.5 5.5 %collective-permute-start.2 = (bf16[1032,128]{1,0:T(8,128)(2,1)S(1)}, bf16[1032,128]{1,0:T(8,128)(2,1)S(1)}, u32[]{:S(2)}, u32[]{:S(2)}) collective-permute-start(bf16[1032,128]{1,0:T(8,128)(2,1)S(1)} %get-tuple-element.30), channel_id=1, source_target_pairs={{0,32},{1,9},{2,34},{3,11},{4,36},{5,13},{6,38},{7,15},{8,40},{9,1... | collective-permute-start | bytes 792584 | tf_op jit(solution)/shard_map/ppermute | solution.py:48
  17.3 20.5 %copy-start = (f32[1024,192]{0,1:T(8,128)S(1)}, f32[1024,192]{0,1:T(8,128)}, u32[]{:S(2)}) copy-start(f32[1024,192]{0,1:T(8,128)} %param.19) | copy-start | bytes 2359300
  17.3 7.2 %collective-permute-start.7 = (bf16[1032,128]{1,0:T(8,128)(2,1)S(1)}, bf16[1032,128]{1,0:T(8,128)(2,1)S(1)}, u32[]{:S(2)}, u32[]{:S(2)}) collective-permute-start(bf16[1032,128]{1,0:T(8,128)(2,1)S(1)} %shard_map.146.refs_0_), channel_id=1, source_target_pairs={{0,16},{1,65},{2,18},{3,67},{4,20},{5,69},{6,22},{7,71},{8,24},{9,... | collective-permute-start | bytes 792584 | tf_op jit(solution)/shard_map/ppermute | solution.py:48
  20.4 6.9 %collective-permute-start.8 = (bf16[1032,128]{1,0:T(8,128)(2,1)S(1)}, bf16[1032,128]{1,0:T(8,128)(2,1)S(1)}, u32[]{:S(2)}, u32[]{:S(2)}) collective-permute-start(bf16[1032,128]{1,0:T(8,128)(2,1)S(1)} %shard_map.146.refs_0_), channel_id=1, source_target_pairs={{0,24},{1,97},{2,26},{3,99},{4,28},{5,101},{6,30},{7,103},{8,16},{... | collective-permute-start | bytes 792584 | tf_op jit(solution)/shard_map/ppermute | solution.py:48
  20.9 7.4 %collective-permute-start.9 = (bf16[1032,128]{1,0:T(8,128)(2,1)S(1)}, bf16[1032,128]{1,0:T(8,128)(2,1)S(1)}, u32[]{:S(2)}, u32[]{:S(2)}) collective-permute-start(bf16[1032,128]{1,0:T(8,128)(2,1)S(1)} %shard_map.146.refs_0_), channel_id=1, source_target_pairs={{0,8},{1,33},{2,10},{3,35},{4,12},{5,37},{6,14},{7,39},{8,0},{9,41... | collective-permute-start | bytes 792584 | tf_op jit(solution)/shard_map/ppermute | solution.py:48
  28.3 18.9 %copy-start.4 = (f32[192]{0:T(256)S(1)}, f32[192]{0:T(256)}, u32[]{:S(2)}) copy-start(f32[192]{0:T(256)} %param.22) | copy-start | bytes 2308
  28.7 4.0 %collective-permute-start.10 = (bf16[64,1024]{1,0:T(8,128)(2,1)S(1)}, bf16[64,1024]{1,0:T(8,128)(2,1)S(1)}, u32[]{:S(2)}, u32[]{:S(2)}) collective-permute-start(bf16[64,1024]{1,0:T(8,128)(2,1)S(1)} %shard_map.147.refs_0_), channel_id=1, source_target_pairs={{0,32},{1,9},{2,34},{3,11},{4,36},{5,13},{6,38},{7,15},{8,40},{9,1... | collective-permute-start | bytes 393224 | tf_op jit(solution)/shard_map/ppermute | solution.py:48
  30.1 6.4 %collective-permute-start.11 = (bf16[64,1024]{1,0:T(8,128)(2,1)S(1)}, bf16[64,1024]{1,0:T(8,128)(2,1)S(1)}, u32[]{:S(2)}, u32[]{:S(2)}) collective-permute-start(bf16[64,1024]{1,0:T(8,128)(2,1)S(1)} %shard_map.147.refs_0_), channel_id=1, source_target_pairs={{0,64},{1,17},{2,66},{3,19},{4,68},{5,21},{6,70},{7,23},{8,72},{9,... | collective-permute-start | bytes 393224 | tf_op jit(solution)/shard_map/ppermute | solution.py:48
  32.7 5.2 %collective-permute-start.12 = (bf16[64,1024]{1,0:T(8,128)(2,1)S(1)}, bf16[64,1024]{1,0:T(8,128)(2,1)S(1)}, u32[]{:S(2)}, u32[]{:S(2)}) collective-permute-start(bf16[64,1024]{1,0:T(8,128)(2,1)S(1)} %shard_map.147.refs_0_), channel_id=1, source_target_pairs={{0,96},{1,25},{2,98},{3,27},{4,100},{5,29},{6,102},{7,31},{8,104},... | collective-permute-start | bytes 393224 | tf_op jit(solution)/shard_map/ppermute | solution.py:48
  37.8 13.1 %copy-start.2 = (f32[192,1024]{1,0:T(8,128)S(1)}, f32[192,1024]{1,0:T(8,128)}, u32[]{:S(2)}) copy-start(f32[192,1024]{1,0:T(8,128)} %refs_0_.1) | copy-start | bytes 2359300
  37.8 13.1 %copy-start.3 = (f32[192,1024]{1,0:T(8,128)S(1)}, f32[192,1024]{1,0:T(8,128)}, u32[]{:S(2)}) copy-start(f32[192,1024]{1,0:T(8,128)} %refs_2_.1) | copy-start | bytes 2359300
  38.3 5.2 %collective-permute-start.13 = (bf16[192,128]{1,0:T(8,128)(2,1)S(1)}, bf16[192,128]{1,0:T(8,128)(2,1)S(1)}, u32[]{:S(2)}, u32[]{:S(2)}) collective-permute-start(bf16[192,128]{1,0:T(8,128)(2,1)S(1)} %get-tuple-element.37), channel_id=1, source_target_pairs={{0,1},{1,0},{2,3},{3,2},{4,5},{5,4},{6,7},{7,6},{8,9},{9,8},{10,11... | collective-permute-start | bytes 147464 | tf_op jit(solution)/shard_map/ppermute | solution.py:52
  43.5 4.5 %collective-permute-start.14 = (bf16[192,128]{1,0:T(8,128)(2,1)S(1)}, bf16[192,128]{1,0:T(8,128)(2,1)S(1)}, u32[]{:S(2)}, u32[]{:S(2)}) collective-permute-start(bf16[192,128]{1,0:T(8,128)(2,1)S(1)} %fusion.1), channel_id=1, source_target_pairs={{0,4},{1,5},{2,6},{3,7},{4,0},{5,1},{6,2},{7,3},{8,12},{9,13},{10,... | collective-permute-start | bytes 147464 | tf_op jit(solution)/shard_map/ppermute | solution.py:58
  46.3 3.1 %collective-permute-start.15 = (bf16[192,128]{1,0:T(8,128)(2,1)S(1)}, bf16[192,128]{1,0:T(8,128)(2,1)S(1)}, u32[]{:S(2)}, u32[]{:S(2)}) collective-permute-start(bf16[192,128]{1,0:T(8,128)(2,1)S(1)} %fusion.1), channel_id=1, source_target_pairs={{0,2},{1,3},{2,0},{3,1},{4,6},{5,7},{6,4},{7,5},{8,10},{9,11},{10,... | collective-permute-start | bytes 147464 | tf_op jit(solution)/shard_map/ppermute | solution.py:58
  46.6 4.2 %collective-permute-start.16 = (bf16[192,128]{1,0:T(8,128)(2,1)S(1)}, bf16[192,128]{1,0:T(8,128)(2,1)S(1)}, u32[]{:S(2)}, u32[]{:S(2)}) collective-permute-start(bf16[192,128]{1,0:T(8,128)(2,1)S(1)} %fusion.1), channel_id=1, source_target_pairs={{0,6},{1,7},{2,4},{3,5},{4,2},{5,3},{6,0},{7,1},{8,14},{9,15},{10,... | collective-permute-start | bytes 147464 | tf_op jit(solution)/shard_map/ppermute | solution.py:58
  51.4 7.1 %collective-permute-start.17 = (bf16[1032,128]{1,0:T(8,128)(2,1)S(1)}, bf16[1032,128]{1,0:T(8,128)(2,1)S(1)}, u32[]{:S(2)}, u32[]{:S(2)}) collective-permute-start(bf16[1032,128]{1,0:T(8,128)(2,1)S(1)} %get-tuple-element.42), channel_id=1, source_target_pairs={{0,64},{1,17},{2,66},{3,19},{4,68},{5,21},{6,70},{7,23},{8,72},{9,... | collective-permute-start | bytes 792584 | tf_op jit(solution)/shard_map/ppermute | solution.py:48
  53.3 8.1 %collective-permute-start.18 = (bf16[1032,128]{1,0:T(8,128)(2,1)S(1)}, bf16[1032,128]{1,0:T(8,128)(2,1)S(1)}, u32[]{:S(2)}, u32[]{:S(2)}) collective-permute-start(bf16[1032,128]{1,0:T(8,128)(2,1)S(1)} %get-tuple-element.43), channel_id=1, source_target_pairs={{0,96},{1,25},{2,98},{3,27},{4,100},{5,29},{6,102},{7,31},{8,104},... | collective-permute-start | bytes 792584 | tf_op jit(solution)/shard_map/ppermute | solution.py:48
  55.0 6.4 %collective-permute-start.19 = (bf16[1032,128]{1,0:T(8,128)(2,1)S(1)}, bf16[1032,128]{1,0:T(8,128)(2,1)S(1)}, u32[]{:S(2)}, u32[]{:S(2)}) collective-permute-start(bf16[1032,128]{1,0:T(8,128)(2,1)S(1)} %get-tuple-element.44), channel_id=1, source_target_pairs={{0,32},{1,9},{2,34},{3,11},{4,36},{5,13},{6,38},{7,15},{8,40},{9,1... | collective-permute-start | bytes 792584 | tf_op jit(solution)/shard_map/ppermute | solution.py:48
  61.7 18.9 %copy-start.1 = (f32[1024,192]{0,1:T(8,128)S(1)}, f32[1024,192]{0,1:T(8,128)}, u32[]{:S(2)}) copy-start(f32[1024,192]{0,1:T(8,128)} %param.26) | copy-start | bytes 2359300
  61.7 6.9 %collective-permute-start.20 = (bf16[1032,128]{1,0:T(8,128)(2,1)S(1)}, bf16[1032,128]{1,0:T(8,128)(2,1)S(1)}, u32[]{:S(2)}, u32[]{:S(2)}) collective-permute-start(bf16[1032,128]{1,0:T(8,128)(2,1)S(1)} %shard_map.150.refs_0_), channel_id=1, source_target_pairs={{0,16},{1,65},{2,18},{3,67},{4,20},{5,69},{6,22},{7,71},{8,24},{9,... | collective-permute-start | bytes 792584 | tf_op jit(solution)/shard_map/ppermute | solution.py:48
  61.8 9.6 %collective-permute-start.21 = (bf16[1032,128]{1,0:T(8,128)(2,1)S(1)}, bf16[1032,128]{1,0:T(8,128)(2,1)S(1)}, u32[]{:S(2)}, u32[]{:S(2)}) collective-permute-start(bf16[1032,128]{1,0:T(8,128)(2,1)S(1)} %shard_map.150.refs_0_), channel_id=1, source_target_pairs={{0,24},{1,97},{2,26},{3,99},{4,28},{5,101},{6,30},{7,103},{8,16},{... | collective-permute-start | bytes 792584 | tf_op jit(solution)/shard_map/ppermute | solution.py:48
  63.3 8.2 %collective-permute-start.22 = (bf16[1032,128]{1,0:T(8,128)(2,1)S(1)}, bf16[1032,128]{1,0:T(8,128)(2,1)S(1)}, u32[]{:S(2)}, u32[]{:S(2)}) collective-permute-start(bf16[1032,128]{1,0:T(8,128)(2,1)S(1)} %shard_map.150.refs_0_), channel_id=1, source_target_pairs={{0,8},{1,33},{2,10},{3,35},{4,12},{5,37},{6,14},{7,39},{8,0},{9,41... | collective-permute-start | bytes 792584 | tf_op jit(solution)/shard_map/ppermute | solution.py:48
  71.8 12.6 %copy-start.5 = (f32[192]{0:T(256)S(1)}, f32[192]{0:T(256)}, u32[]{:S(2)}) copy-start(f32[192]{0:T(256)} %param.29) | copy-start | bytes 2308
  71.8 4.3 %collective-permute-start.23 = (bf16[32,2048]{1,0:T(8,128)(2,1)S(1)}, bf16[32,2048]{1,0:T(8,128)(2,1)S(1)}, u32[]{:S(2)}, u32[]{:S(2)}) collective-permute-start(bf16[32,2048]{1,0:T(8,128)(2,1)S(1)} %shard_map.151.refs_0_), channel_id=1, source_target_pairs={{0,32},{1,9},{2,34},{3,11},{4,36},{5,13},{6,38},{7,15},{8,40},{9,1... | collective-permute-start | bytes 393224 | tf_op jit(solution)/shard_map/ppermute | solution.py:48
  72.8 6.4 %collective-permute-start.24 = (bf16[32,2048]{1,0:T(8,128)(2,1)S(1)}, bf16[32,2048]{1,0:T(8,128)(2,1)S(1)}, u32[]{:S(2)}, u32[]{:S(2)}) collective-permute-start(bf16[32,2048]{1,0:T(8,128)(2,1)S(1)} %shard_map.151.refs_0_), channel_id=1, source_target_pairs={{0,64},{1,17},{2,66},{3,19},{4,68},{5,21},{6,70},{7,23},{8,72},{9,... | collective-permute-start | bytes 393224 | tf_op jit(solution)/shard_map/ppermute | solution.py:48
  75.5 5.2 %collective-permute-start.25 = (bf16[32,2048]{1,0:T(8,128)(2,1)S(1)}, bf16[32,2048]{1,0:T(8,128)(2,1)S(1)}, u32[]{:S(2)}, u32[]{:S(2)}) collective-permute-start(bf16[32,2048]{1,0:T(8,128)(2,1)S(1)} %shard_map.151.refs_0_), channel_id=1, source_target_pairs={{0,96},{1,25},{2,98},{3,27},{4,100},{5,29},{6,102},{7,31},{8,104},... | collective-permute-start | bytes 393224 | tf_op jit(solution)/shard_map/ppermute | solution.py:48
  81.1 4.5 %collective-permute-start.26 = (bf16[192,128]{1,0:T(8,128)(2,1)S(1)}, bf16[192,128]{1,0:T(8,128)(2,1)S(1)}, u32[]{:S(2)}, u32[]{:S(2)}) collective-permute-start(bf16[192,128]{1,0:T(8,128)(2,1)S(1)} %shard_map.152), channel_id=1, source_target_pairs={{0,4},{1,5},{2,6},{3,7},{4,0},{5,1},{6,2},{7,3},{8,12},{9,13},{10,... | collective-permute-start | bytes 147464 | tf_op jit(solution)/shard_map/ppermute | solution.py:58
  82.5 3.1 %collective-permute-start.27 = (bf16[192,128]{1,0:T(8,128)(2,1)S(1)}, bf16[192,128]{1,0:T(8,128)(2,1)S(1)}, u32[]{:S(2)}, u32[]{:S(2)}) collective-permute-start(bf16[192,128]{1,0:T(8,128)(2,1)S(1)} %shard_map.152), channel_id=1, source_target_pairs={{0,2},{1,3},{2,0},{3,1},{4,6},{5,7},{6,4},{7,5},{8,10},{9,11},{10,... | collective-permute-start | bytes 147464 | tf_op jit(solution)/shard_map/ppermute | solution.py:58
  83.1 4.2 %collective-permute-start.28 = (bf16[192,128]{1,0:T(8,128)(2,1)S(1)}, bf16[192,128]{1,0:T(8,128)(2,1)S(1)}, u32[]{:S(2)}, u32[]{:S(2)}) collective-permute-start(bf16[192,128]{1,0:T(8,128)(2,1)S(1)} %shard_map.152), channel_id=1, source_target_pairs={{0,6},{1,7},{2,4},{3,5},{4,2},{5,3},{6,0},{7,1},{8,14},{9,15},{10,... | collective-permute-start | bytes 147464 | tf_op jit(solution)/shard_map/ppermute | solution.py:58
  87.3 5.2 %collective-permute-start.29 = (bf16[192,128]{1,0:T(8,128)(2,1)S(1)}, bf16[192,128]{1,0:T(8,128)(2,1)S(1)}, u32[]{:S(2)}, u32[]{:S(2)}) collective-permute-start(bf16[192,128]{1,0:T(8,128)(2,1)S(1)} %add_convert_fusion), channel_id=1, source_target_pairs={{0,1},{1,0},{2,3},{3,2},{4,5},{5,4},{6,7},{7,6},{8,9},{9,8},{10,11... | collective-permute-start | bytes 147464 | tf_op jit(solution)/shard_map/ppermute | solution.py:52
